TPU v7x, 768 devices: a whole 4x8x12 slice. The times are simulated.
768 devices in a mesh: sp: 16 (over y, core), dp: 48 (over z, x).
Axes of the slice: x: 4, y: 8, z: 12, core: 2. Of those that a mesh axis runs over, the one named last changes fastest.
Arguments:
- standardized_block_source: bfloat16 [96, 1024, 2064], P('dp', 'sp'), may hold values from -6 to 6
- forgetting_narrowing_matrix: bfloat16 [2064, 32], P('dp'), may hold values from -0.125 to 0.125
- forgetting_widening_matrix: bfloat16 [32, 1024], replicated, may hold values from -1 to 1
- forgetting_offset_vector: float32 [1024], replicated, may hold values from -1.5 to 6.5
- probe_vectors: bfloat16 [768, 1024, 128], P(('dp', 'sp')), may hold values from -6 to 6
- address_vectors: bfloat16 [768, 1024, 128], P(('dp', 'sp')), may hold values from -6 to 6
- payload_vectors: bfloat16 [768, 1024, 256], P(('dp', 'sp')), may hold values from -6 to 6
- extra_channel_forgetting: float32 [768, 1024], P(('dp', 'sp')), may hold values from -2.1 to 0
- blender_result_adjoint: bfloat16 [96, 1024, 2048], P('dp', 'sp'), may hold values from -0.29882812 to 0.29882812
Outputs:
- grad_queries: bfloat16 [96, 1024, 1024], P('dp', 'sp')
- grad_keys: bfloat16 [96, 1024, 1024], P('dp', 'sp')
- grad_values: bfloat16 [96, 1024, 2048], P('dp', 'sp')
- grad_input: bfloat16 [96, 1024, 2064], P('dp', 'sp')
- grad_gate_down: float32 [2064, 32], P('dp')
- grad_gate_up: float32 [32, 1024], replicated
- grad_gate_bias: float32 [1024], replicated
All inputs are finite; a program needn't handle non-finite values.
Results may differ from a plain program's by a relative error of at most 0.0069.
Values may be sent and summed in bfloat16 or wider, within the bound.
No kernel may reach another device: no remote copies, remote signals or barrier semaphores. Data moves between devices by JAX's collectives and lax.ppermute only.
A program may use at most 32 MiB of HBM per device.

v0:
```python
import jax
import jax.numpy as jnp
from jax import lax
from jax.sharding import PartitionSpec as P

HEADS = 8
ADDRESS_WIDTH = 128
PAYLOAD_WIDTH = 256
RANK = 32
BLOCK = 64


retention_smoothing = 16.0


def joined_along(parts, dim):
    lengths = list(parts.shape[1:])
    lengths[dim] *= parts.shape[0]
    return jnp.moveaxis(parts, 0, dim).reshape(lengths)


def from_everyone(shard, axis):
    copies = jnp.broadcast_to(shard, (lax.axis_size(axis), *shard.shape))
    return lax.all_to_all(copies, axis, split_axis=0, concat_axis=0, tiled=True)


def gather_directly(shard, axis, dim):
    return joined_along(from_everyone(shard, axis), dim)


def side_by_side(arrays, axis, split_dim, concat_dim, along):
    both = jnp.concatenate(arrays, axis=along)
    out, at, outs = (
        lax.all_to_all(both, axis, split_axis=split_dim, concat_axis=concat_dim, tiled=True),
        0,
        [],
    )
    for a in arrays:
        outs.append(lax.slice_in_dim(out, at, at + a.shape[along], axis=along))
        at += a.shape[along]
    return tuple(outs)


def in_one(arrays, axis):
    vector, at, outs = (jnp.concatenate([a.reshape(-1) for a in arrays]), 0, [])
    running = lax.psum(vector, axis)
    for a in arrays:
        outs.append(running[at : at + a.size].reshape(a.shape))
        at += a.size
    return tuple(outs)


def head_forward(
    stream_probe_entries, stream_address_entries, stream_payload_entries, retention_coefficient
):
    length, key_width = stream_probe_entries.shape
    value_width = stream_payload_entries.shape[1]
    blocks = length // BLOCK
    middle = BLOCK // 2
    scaled = stream_probe_entries * key_width ** (-0.5)
    causal = jnp.tril(jnp.ones((BLOCK, BLOCK), dtype=bool))
    highest = lax.Precision.HIGHEST

    def advance(memory, pieces):
        query_block, key_block, value_block, decay_sums = pieces
        centre = decay_sums[middle]
        lifted_query = query_block * jnp.exp(decay_sums - centre[None, :])
        lowered_key = key_block * jnp.exp(centre[None, :] - decay_sums)
        raw_scores = jnp.dot(lifted_query, lowered_key.T, precision=highest)
        scores = jnp.where(causal, raw_scores, 0.0)
        within = jnp.dot(scores, value_block, precision=highest)
        carried = jnp.dot(query_block * jnp.exp(decay_sums), memory, precision=highest)
        ending = decay_sums[-1]
        fading = key_block * jnp.exp(ending[None, :] - decay_sums)
        memory = memory * jnp.exp(ending)[:, None] + jnp.dot(
            fading.T, value_block, precision=highest
        )
        return (memory, within + carried)

    def blocked(tensor):
        return tensor.reshape(blocks, BLOCK, tensor.shape[1])

    initial = jnp.zeros((key_width, value_width), jnp.float32)
    decay_sums = jnp.cumsum(blocked(retention_coefficient), axis=1)
    _, outputs = lax.scan(
        jax.checkpoint(advance),
        initial,
        (
            blocked(scaled),
            blocked(stream_address_entries),
            blocked(stream_payload_entries),
            decay_sums,
        ),
    )
    return outputs.reshape(length, value_width)


def stream_sensitivities(
    stream_probe_entries,
    stream_address_entries,
    stream_payload_entries,
    forgetting_logit_values,
    surplus_retention_loss,
    result_adjoint,
):

    def forward(query_in, key_in, value_in, retention_basis_components):
        retention_coefficient = (
            jax.nn.log_sigmoid(retention_basis_components) / retention_smoothing
            + surplus_retention_loss[:, None]
        )
        return head_forward(query_in, key_in, value_in, retention_coefficient)

    _, pullback = jax.vjp(
        forward,
        stream_probe_entries.astype(jnp.float32),
        stream_address_entries.astype(jnp.float32),
        stream_payload_entries.astype(jnp.float32),
        forgetting_logit_values,
    )
    query_grad, key_grad, value_grad, gate_grad = pullback(result_adjoint.astype(jnp.float32))
    return (
        query_grad.astype(jnp.bfloat16),
        key_grad.astype(jnp.bfloat16),
        value_grad.astype(jnp.bfloat16),
        gate_grad.astype(jnp.bfloat16),
    )


def on_device(
    standardized_block_source,
    forgetting_narrowing_matrix,
    forgetting_widening_matrix,
    forgetting_offset_vector,
    probe_vectors,
    address_vectors,
    payload_vectors,
    extra_channel_forgetting,
    blender_result_adjoint,
):
    seqs, local_len, model_width = standardized_block_source.shape
    tokens_dev = seqs * local_len
    items = probe_vectors.shape[0]
    contract = (((0,), (0,)), ((), ()))
    flat_input = standardized_block_source.reshape(tokens_dev, model_width)
    down_whole = gather_directly(forgetting_narrowing_matrix, "dp", 0)
    low_rank = jnp.dot(flat_input, down_whole, preferred_element_type=jnp.float32).astype(
        jnp.bfloat16
    )
    low_all = gather_directly(low_rank.reshape(seqs, local_len, RANK), "sp", 1)
    figures_list = lax.axis_index("sp") * items + jnp.arange(items, dtype=jnp.int32)

    def head_gate(number):
        head_start = number % HEADS * ADDRESS_WIDTH
        seq_low = lax.dynamic_index_in_dim(low_all, number // HEADS, 0, keepdims=False)
        columns = lax.dynamic_slice_in_dim(forgetting_widening_matrix, head_start, ADDRESS_WIDTH, 1)
        offsets = lax.dynamic_slice_in_dim(forgetting_offset_vector, head_start, ADDRESS_WIDTH, 0)
        return jnp.dot(seq_low, columns, preferred_element_type=jnp.float32) + offsets

    logit_by_stream = jax.vmap(head_gate)(figures_list)
    cot_items = (
        blender_result_adjoint.reshape(seqs, local_len, HEADS, PAYLOAD_WIDTH)
        .transpose(0, 2, 1, 3)
        .reshape(seqs * HEADS, local_len, PAYLOAD_WIDTH)
    )
    adjoint_split_by_stream = lax.all_to_all(
        cot_items, "sp", split_axis=0, concat_axis=1, tiled=True
    )
    query_grad, key_grad, value_grad, gate_grad = jax.vmap(stream_sensitivities)(
        probe_vectors,
        address_vectors,
        payload_vectors,
        logit_by_stream,
        extra_channel_forgetting,
        adjoint_split_by_stream,
    )
    returned = side_by_side((query_grad, key_grad, value_grad, gate_grad), "sp", 1, 0, 2)

    def to_tokens(tensor):
        columns = tensor.shape[2]
        return (
            tensor.reshape(seqs, HEADS, local_len, columns)
            .transpose(0, 2, 1, 3)
            .reshape(seqs, local_len, HEADS * columns)
        )

    gate_tokens = to_tokens(returned[3]).reshape(tokens_dev, HEADS * ADDRESS_WIDTH)
    low_grad = jnp.dot(
        gate_tokens, forgetting_widening_matrix.T, preferred_element_type=jnp.float32
    ).astype(jnp.bfloat16)
    incoming_sensitivity = jnp.dot(
        low_grad, down_whole.T, preferred_element_type=jnp.float32
    ).astype(jnp.bfloat16)
    up_term = lax.dot_general(low_rank, gate_tokens, contract, preferred_element_type=jnp.float32)
    bias_term = jnp.sum(gate_tokens.astype(jnp.float32), axis=0)
    partition_lines_count = forgetting_narrowing_matrix.shape[0]
    whole_term = lax.dot_general(flat_input, low_grad, contract, preferred_element_type=jnp.float32)
    combined_contraction, up_grad, bias_grad = in_one(
        (whole_term, up_term, bias_term), ("sp", "dp")
    )
    down_grad = lax.dynamic_slice_in_dim(
        combined_contraction, lax.axis_index("dp") * partition_lines_count, partition_lines_count, 0
    )
    return (
        to_tokens(returned[0]),
        to_tokens(returned[1]),
        to_tokens(returned[2]),
        incoming_sensitivity.reshape(seqs, local_len, model_width),
        down_grad,
        up_grad,
        bias_grad,
    )


def solution(mesh):
    placed = (
        P("dp", "sp", None),
        P("dp", None),
        P(),
        P(),
        P(("dp", "sp"), None, None),
        P(("dp", "sp"), None, None),
        P(("dp", "sp"), None, None),
        P(("dp", "sp"), None),
        P("dp", "sp", None),
    )
    return jax.shard_map(
        on_device,
        mesh=mesh,
        in_specs=placed,
        out_specs=(
            P("dp", "sp", None),
            P("dp", "sp", None),
            P("dp", "sp", None),
            P("dp", "sp", None),
            P("dp", None),
            P(),
            P(),
        ),
        check_vma=False,
    )
```

profile of v0, /device:TPU:1, one launch (start us, length us, event | category | flops | bytes accessed | tf_op | source)
XLA Modules:
  0.0 761.9 jit_solution(3889222509544817573)
XLA Ops:
  8.0 1.2 reshape.603
  9.2 19.0 %all-to-all-start = ((bf16[48,2,688]{2,1,0:T(2,128)(2,1)}), bf16[48,2,688]{2,1,0:T(2,128)(2,1)S(1)}, u32[]{:S(2)}, u32[]{:S(2)}) async-start(bf16[48,2,688]{2,1,0:T(2,128)(2,1)} %reshape.603), calls=%async_computation | async-start | bytes 294912 | tf_op jit(solution)/shard_map/all_to_all | solution.py:24
  28.9 12.0 %all-to-all-done = bf16[48,2,688]{2,1,0:T(2,128)(2,1)S(1)} async-done(((bf16[48,2,688]{2,1,0:T(2,128)(2,1)}), bf16[48,2,688]{2,1,0:T(2,128)(2,1)S(1)}, u32[]{:S(2)}, u32[]{:S(2)}) %all-to-all-start) | async-done | bytes 132128 | tf_op jit(solution)/shard_map/all_to_all | solution.py:24
  43.5 9.5 %all-to-all-start.1 = ((bf16[16,2,2048]{2,1,0:T(2,128)(2,1)}), bf16[16,2,2048]{2,1,0:T(2,128)(2,1)S(1)}, u32[]{:S(2)}, u32[]{:S(2)}) async-start(bf16[16,2,2048]{2,1,0:T(2,128)(2,1)} %reshape.605), calls=%async_computation.1 | async-start | bytes 262144 | tf_op jit(solution)/shard_map/all_to_all | solution.py:24
  56.5 5.4 all-to-all-done.1
  62.0 3.5 all-to-all-start.2
  66.1 1.3 multiply_add_fusion
  67.9 29.6 %while.39 = (s32[]{:T(128)}, f32[1,128,256]{2,1,0:T(8,128)S(1)}, f32[16,1,128,256]{3,2,1,0:T(8,128)}, f32[16,1,64,128]{3,2,1,0:T(8,128)S(1)}, f32[16,1,64,128]{3...) while((s32[]{:T(128)}, f32[1,128,256]{2,1,0:T(8,128)S(1)}, ...), condition=%wide.region_2.3_spmd.clone, body=%wide.region_1.2_spmd.clone.sunk | while | flops 25313284 | bytes 725615 | solution.py:85
  68.6 1.1 fusion.106
  70.4 1.1 fusion.106
  72.3 1.1 fusion.106
  74.1 1.1 fusion.106
  76.0 1.1 fusion.106
  77.8 1.1 fusion.106
  79.6 1.1 fusion.106
  81.5 1.1 fusion.106
  83.3 1.1 fusion.106
  85.2 1.1 fusion.106
  87.0 1.1 fusion.106
  90.7 1.1 fusion.106
  92.6 1.1 fusion.106
  94.4 1.1 fusion.106
  99.5 131.6 %while.40 = (s32[]{:T(128)}, f32[1,128,256]{1,2,0:T(8,128)S(1)}, f32[16,1,64,128]{3,2,1,0:T(8,128)S(1)}, bf16[16,1,64,128]{3,2,1,0:T(8,128)(2,1)}, bf16[16,1,64,...) while((s32[]{:T(128)}, f32[1,128,256]{1,2,0:T(8,128)S(1)}, ...), condition=%wide.region_8.9_spmd.clone, body=%wide.region_3.8_spmd.clone.sunk | while | flops 145305600 | bytes 4107463 | solution.py:85
  106.0 1.7 dynamic_update_slice.58
  114.2 1.7 dynamic_update_slice.58
  122.4 1.7 dynamic_update_slice.58
  130.7 1.7 dynamic_update_slice.58
  138.9 1.7 dynamic_update_slice.58
  147.1 1.7 dynamic_update_slice.58
  155.3 1.7 dynamic_update_slice.58
  163.6 1.7 dynamic_update_slice.58
  171.8 1.7 dynamic_update_slice.58
  180.0 1.7 dynamic_update_slice.58
  188.2 1.7 dynamic_update_slice.58
  196.4 1.7 dynamic_update_slice.58
  204.7 1.7 dynamic_update_slice.58
  212.9 1.7 dynamic_update_slice.58
  221.1 1.7 dynamic_update_slice.58
  229.3 1.7 dynamic_update_slice.58
  231.1 1.7 multiply_negate_fusion
  233.6 2.0 copy.121
  236.2 9.9 %reduce.29 = bf16[1024,640]{1,0:T(8,128)(2,1)} reduce(bf16[1024,1,640]{2,1,0:T(2,128)(2,1)S(1)} %bitcast.310, bf16[]{:T(256)} %broadcast.156), dimensions={1}, to_apply=%bitcast.223.reduce_sub_computation | reduce | bytes 2621442
  246.1 4.1 reshape.607
  250.1 7.0 all-to-all-start.3
  257.2 33.3 %all-to-all-done.3 = bf16[16,2,20480]{2,1,0:T(2,128)(2,1)} async-done(((bf16[16,2,20480]{2,1,0:T(2,128)(2,1)}), bf16[16,2,20480]{2,1,0:T(2,128)(2,1)}, u32[]{:S(2)}, u32[]{:S(2)}) %all-to-all-start.3) | async-done | bytes 1310752 | tf_op jit(solution)/shard_map/all_to_all | solution.py:34
  290.5 4.5 reshape.608
  301.0 449.2 %all-reduce.5.cloned.1.call-done = f32[99840]{0:T(1024)} async-done(((f32[99840]{0:T(1024)}), f32[99840]{0:T(1024)}) %all-reduce.5.cloned.1.call-update) | async-done | bytes 399376 | tf_op jit(solution)/shard_map/psum | solution.py:46
  753.7 1.3 slice.101
  (512 shorter events, 136.4 us)
Async XLA Ops:
  7.2 35.0 %copy-start = (bf16[2,64,2064]{2,1,0:T(8,128)(2,1)S(1)}, bf16[2,64,2064]{2,1,0:T(8,128)(2,1)}, u32[]{:S(2)}) copy-start(bf16[2,64,2064]{2,1,0:T(8,128)(2,1)} %param.13) | copy-start | bytes 1585156
  9.2 43.9 %copy-start.6 = (bf16[1,1024,128]{2,1,0:T(8,128)(2,1)S(1)}, bf16[1,1024,128]{2,1,0:T(8,128)(2,1)}, u32[]{:S(2)}) copy-start(bf16[1,1024,128]{2,1,0:T(8,128)(2,1)} %param.18) | copy-start | bytes 786436
  9.2 31.8 %all-to-all-start = ((bf16[48,2,688]{2,1,0:T(2,128)(2,1)}), bf16[48,2,688]{2,1,0:T(2,128)(2,1)S(1)}, u32[]{:S(2)}, u32[]{:S(2)}) async-start(bf16[48,2,688]{2,1,0:T(2,128)(2,1)} %reshape.603), calls=%async_computation | async-start | bytes 294912 | tf_op jit(solution)/shard_map/all_to_all | solution.py:24
  28.9 25.0 %copy-start.3 = (bf16[1,1024,256]{2,1,0:T(8,128)(2,1)S(1)}, bf16[1,1024,256]{2,1,0:T(8,128)(2,1)}, u32[]{:S(2)}) copy-start(bf16[1,1024,256]{2,1,0:T(8,128)(2,1)} %param.19) | copy-start | bytes 1572868
  42.1 11.9 %copy-start.4 = (bf16[2,64,2048]{2,1,0:T(8,128)(2,1)S(1)}, bf16[2,64,2048]{2,1,0:T(8,128)(2,1)}, u32[]{:S(2)}) copy-start(bf16[2,64,2048]{2,1,0:T(8,128)(2,1)} %param.21) | copy-start | bytes 1572868
  42.6 13.1 %copy-start.7 = (bf16[1,1024,128]{2,1,0:T(8,128)(2,1)S(1)}, bf16[1,1024,128]{2,1,0:T(8,128)(2,1)}, u32[]{:S(2)}) copy-start(bf16[1,1024,128]{2,1,0:T(8,128)(2,1)} %param.17) | copy-start | bytes 786436
  43.5 18.4 %all-to-all-start.1 = ((bf16[16,2,2048]{2,1,0:T(2,128)(2,1)}), bf16[16,2,2048]{2,1,0:T(2,128)(2,1)S(1)}, u32[]{:S(2)}, u32[]{:S(2)}) async-start(bf16[16,2,2048]{2,1,0:T(2,128)(2,1)} %reshape.605), calls=%async_computation.1 | async-start | bytes 262144 | tf_op jit(solution)/shard_map/all_to_all | solution.py:24
  54.9 11.2 %copy-start.8 = (bf16[32,1024]{1,0:T(8,128)(2,1)S(1)}, bf16[32,1024]{1,0:T(8,128)(2,1)}, u32[]{:S(2)}) copy-start(bf16[32,1024]{1,0:T(8,128)(2,1)} %param.15) | copy-start | bytes 196612
  54.9 11.2 %copy-start.9 = (f32[1,1024]{1,0:T(1,128)S(1)}, f32[1,1024]{1,0:T(1,128)}, u32[]{:S(2)}) copy-start(f32[1,1024]{1,0:T(1,128)} %param.20) | copy-start | bytes 12292
  62.0 35.5 %all-to-all-start.2 = ((bf16[16,64,256]{2,1,0:T(8,128)(2,1)}), bf16[16,64,256]{2,1,0:T(8,128)(2,1)S(1)}, u32[]{:S(2)}, u32[]{:S(2)}) async-start(bf16[16,64,256]{2,1,0:T(8,128)(2,1)} %bitcast.12), calls=%async_computation.2 | async-start | bytes 1048576 | tf_op jit(solution)/shard_map/all_to_all | solution.py:166
  97.4 1.2 copy-start.1
  231.1 1.9 copy-start.5
  231.1 2.4 copy-start.2
  250.1 40.4 %all-to-all-start.3 = ((bf16[16,2,20480]{2,1,0:T(2,128)(2,1)}), bf16[16,2,20480]{2,1,0:T(2,128)(2,1)}, u32[]{:S(2)}, u32[]{:S(2)}) async-start(bf16[16,2,20480]{2,1,0:T(2,128)(2,1)} %reshape.607), calls=%async_computation.3 | async-start | bytes 2621440 | tf_op jit(solution)/shard_map/all_to_all | solution.py:34
  257.2 493.0 %all-reduce.5.cloned.1.call-start = ((), (), s32[]{:S(2)}) async-start(), calls=%async_computation.4 | async-start | bytes 802816 | tf_op jit(solution)/shard_map/psum | solution.py:46
Sparse Core Ops, SparseCore 0:
  300.2 449.9 all-reduce.4
where the time goes:
time: 767 us; the launch traced here: 762 us
  waiting for transfers between devices  500 us (65%)
  local copies, waits for them, and re-layouts  110 us (14%)
  matrix products  65 us (8%)
  starting transfers between devices  39 us (5%)
  other arithmetic  30.7 us (4%)
  between operations  14.4 us (2%)
    psum x1, waiting for transfers between devices, in_one(): running = lax.psum(vector, axis)  449 us
    squeeze x64, local copies, waits for them, and re-layouts, head_forward(): lax.scan(jax.checkpoint(advance), initial, (blocked(scaled), blocked(stre...  38.4 us
    all_to_all x1, waiting for transfers between devices, side_by_side(): lax.all_to_all(both, axis, split_axis=split_dim, concat_axis=concat_dim,...  33.3 us
    all_to_all x2, starting transfers between devices, from_everyone(): return lax.all_to_all(copies, axis, split_axis=0, concat_axis=0, tiled=True)  28.5 us
    dynamic_update_slice x16, local copies, waits for them, and re-layouts, head_forward(): lax.scan(jax.checkpoint(advance), initial, (blocked(scaled), blocked(stre...  27.9 us
    dot_general x48, matrix products, advance(): jnp.dot(fading.T, value_block, precision=highest)  25.8 us
    dot_general x48, matrix products, advance(): raw_scores = jnp.dot(lifted_query, lowered_key.T, precision=highest)  19.6 us
    all_to_all x2, waiting for transfers between devices, from_everyone(): return lax.all_to_all(copies, axis, split_axis=0, concat_axis=0, tiled=True)  17.5 us
  transfers between devices with their start and end apart: 5, of which 4 were waited for; matrix products, arithmetic and copies ran while one was open for 5% of the time, Pallas kernels for 0%

commit v1 on v0

v1 whole, which is shorter than its diff:
```python
import jax
import jax.numpy as jnp
from jax import lax
from jax.experimental import pallas as pl
from jax.experimental.pallas import tpu as pltpu
from jax.sharding import PartitionSpec as P

HEADS = 8
ADDRESS_WIDTH = 128
PAYLOAD_WIDTH = 256
RANK = 32
BLOCK = 64
SMOOTHING = 16.0
SPAN_LIMIT = 80.0
PACK = 4
f32 = jnp.float32
bf16 = jnp.bfloat16


def mm(a, b, ca=1, cb=0):
    return lax.dot_general(a, b, (((ca,), (cb,)), ((), ())), preferred_element_type=f32)


def two_parts(a):
    hi = a.astype(bf16)
    return hi, (a - hi.astype(f32)).astype(bf16)


def three_parts(a):
    hi = a.astype(bf16)
    return hi, *two_parts(a - hi.astype(f32))


def mixer_kernel(
    came_ref, wu_ref, off_ref, ex_ref, q_ref, k_ref, v_ref,
    goes_ref, bias_ref,
    wbig, parts, b_s, pre_s, qp_s, kf_s, st_s, pt_s, dqi_s, dki_s, x_s, y_s, e_s, gate_s,
):
    blocks = q_ref.shape[0]
    rows = BLOCK // PACK
    lanes = ADDRESS_WIDTH
    scale = ADDRESS_WIDTH ** (-0.5)
    middle = BLOCK // 2

    def do_block(n):
        return jnp.concatenate(
            [came_ref[n, BLOCK * i : BLOCK * (i + 1)] for i in range(PAYLOAD_WIDTH // lanes)],
            axis=1,
        )

    row_id = lax.broadcasted_iota(jnp.int32, (BLOCK, BLOCK), 0)
    col_id = lax.broadcasted_iota(jnp.int32, (BLOCK, BLOCK), 1)

    wbig[...] = jnp.zeros(wbig.shape, bf16)
    for p in range(PACK):
        wbig[RANK * p : RANK * (p + 1), lanes * p : lanes * (p + 1)] = wu_ref[...]
    low = came_ref[:, 2 * BLOCK :].reshape(blocks * rows, lanes)
    raw = mm(low, wbig[...])
    offs = off_ref[...]
    for n in range(blocks):
        pre = (
            jnp.concatenate(
                [
                    raw[rows * n : rows * (n + 1), lanes * p : lanes * (p + 1)]
                    for p in range(PACK)
                ],
                axis=0,
            )
            + offs
        )
        pre_s[n] = pre
        decay = (jnp.minimum(pre, 0.0) - jnp.log1p(jnp.exp(-jnp.abs(pre)))) * (
            1.0 / SMOOTHING
        ) + ex_ref[:, n : n + 1]
        for i, part in enumerate(three_parts(decay)):
            parts[BLOCK * i : BLOCK * (i + 1), lanes * n : lanes * (n + 1)] = part
    lower = (row_id >= col_id).astype(bf16)
    sums = mm(jnp.concatenate([lower] * 3, axis=1), parts[: 3 * BLOCK])
    span = jnp.zeros((1, lanes), f32)
    for n in range(blocks):
        b = sums[:, lanes * n : lanes * (n + 1)]
        b_s[n] = b
        centre = b[middle : middle + 1]
        span = jnp.maximum(span, jnp.maximum(b[:1] - centre, centre - b[BLOCK - 1 :]))
    narrow = jnp.max(span) < SPAN_LIMIT

    @pl.when(narrow)
    def _():
        def within(n, carry):
            b = b_s[n]
            centre = b[middle : middle + 1]
            lift = jnp.exp(b - centre)
            drop = jnp.exp(centre - b)
            qc = (q_ref[n].astype(f32) * scale * lift).astype(bf16)
            kc = (k_ref[n].astype(f32) * drop).astype(bf16)
            do = do_block(n)
            v = v_ref[n]
            pt_s[n] = jnp.where(row_id <= col_id, mm(kc, qc, 1, 1), 0.0).astype(bf16)
            dp = jnp.where(row_id >= col_id, mm(do, v, 1, 1), 0.0).astype(bf16)
            dq = mm(dp, kc)
            dk = mm(dp, qc, 0, 0)
            x_s[n] = dq * qc.astype(f32) - dk * kc.astype(f32)
            dqi_s[n] = dq * lift
            dki_s[n] = dk * drop
            return carry

        lax.fori_loop(0, blocks, within, 0, unroll=4)

    @pl.when(jnp.logical_not(narrow))
    def _():
        def within(n, carry):
            b = b_s[n]
            q = q_ref[n].astype(f32) * scale
            dp = mm(do_block(n), v_ref[n], 1, 1)
            at = lax.broadcasted_iota(jnp.int32, (BLOCK, 1), 0)
            dqi_s[n] = jnp.zeros((BLOCK, lanes), f32)
            x_s[n] = jnp.zeros((BLOCK, lanes), f32)

            def one(s, scores):
                here = at == s
                b_row = jnp.sum(jnp.where(here, b, 0.0), axis=0, keepdims=True)
                k_row = jnp.sum(
                    jnp.where(here, k_ref[n].astype(f32), 0.0), axis=0, keepdims=True
                )
                decay = jnp.where(at >= s, jnp.exp(jnp.minimum(b - b_row, 0.0)), 0.0)
                dp_col = jnp.sum(jnp.where(col_id == s, dp, 0.0), axis=1, keepdims=True)
                qd = q * decay
                column = jnp.sum(qd * k_row, axis=1, keepdims=True)
                dq = dp_col * decay * k_row
                dk_row = jnp.sum(dp_col * qd, axis=0, keepdims=True)
                dqi_s[n] = dqi_s[n] + dq
                dki_s[n] = jnp.where(here, dk_row, dki_s[n])
                x_s[n] = x_s[n] + q * dq - jnp.where(here, dk_row * k_row, 0.0)
                return scores + jnp.where(col_id == s, column, 0.0)

            scores = lax.fori_loop(0, BLOCK, one, jnp.zeros((BLOCK, BLOCK), f32))
            pt_s[n] = scores.T.astype(bf16)
            return carry

        lax.fori_loop(0, blocks, within, 0)

    def forward(n, state):
        b = b_s[n]
        last = b[BLOCK - 1 :]
        grow = jnp.exp(b)
        qp = (q_ref[n].astype(f32) * scale * grow).astype(bf16)
        kf = (k_ref[n].astype(f32) * jnp.exp(last - b)).astype(bf16)
        qp_s[n] = qp
        kf_s[n] = kf
        st_s[n] = state
        dq = mm(do_block(n), state.astype(bf16))
        x_s[n] = x_s[n] + qp.astype(f32) * dq
        goes_ref[n, :BLOCK] = ((dqi_s[n] + dq * grow) * scale).astype(bf16)
        return state * jnp.exp(last) + mm(v_ref[n], kf, 0, 0)

    zero = jnp.zeros((PAYLOAD_WIDTH, lanes), f32)
    lax.fori_loop(0, blocks, forward, zero, unroll=4)

    def backward(i, dstate):
        n = blocks - 1 - i
        b = b_s[n]
        last = b[BLOCK - 1 :]
        do = do_block(n)
        ds = dstate.astype(bf16)
        kf = kf_s[n]
        dk = mm(v_ref[n], ds)
        goes_ref[n, BLOCK : 2 * BLOCK] = (dki_s[n] + dk * jnp.exp(last - b)).astype(bf16)
        dv = (mm(pt_s[n], do) + mm(kf, ds, 1, 1)).astype(bf16)
        goes_ref[n, 2 * BLOCK : 3 * BLOCK] = dv[:, :lanes]
        goes_ref[n, 3 * BLOCK : 4 * BLOCK] = dv[:, lanes:]
        y_s[n] = kf.astype(f32) * dk
        fade = jnp.exp(last)
        e_s[n] = fade * jnp.sum(st_s[n] * dstate, axis=0, keepdims=True)
        return dstate * fade + mm(do, qp_s[n], 0, 0)

    lax.fori_loop(0, blocks, backward, zero, unroll=4)

    for n in range(blocks):
        for i, part in enumerate(three_parts(x_s[n])):
            parts[BLOCK * i : BLOCK * (i + 1), lanes * n : lanes * (n + 1)] = part
        for i, part in enumerate(three_parts(y_s[n])):
            parts[BLOCK * (3 + i) : BLOCK * (4 + i), lanes * n : lanes * (n + 1)] = part
    upper = (row_id <= col_id).astype(bf16)
    before = (row_id > col_id).astype(bf16)
    ddecay = mm(jnp.concatenate([upper] * 3 + [before] * 3, axis=1), parts[...])
    bias = jnp.zeros((1, lanes), f32)
    for n in range(blocks):
        pre = pre_s[n]
        e = jnp.exp(-jnp.abs(pre))
        slope = jnp.where(pre >= 0.0, e, 1.0) / (1.0 + e)
        gate = (
            (ddecay[:, lanes * n : lanes * (n + 1)] + e_s[n]) * slope * (1.0 / SMOOTHING)
        ).astype(bf16)
        bias = bias + jnp.sum(gate.astype(f32), axis=0, keepdims=True)
        for p in range(PACK):
            gate_s[rows * n : rows * (n + 1), lanes * p : lanes * (p + 1)] = gate[
                rows * p : rows * (p + 1)
            ]
    gates = gate_s[...]
    lowg = mm(gates, wbig[...], 1, 1)
    goes_ref[:, 4 * BLOCK : 4 * BLOCK + rows] = lowg.reshape(blocks, rows, lanes).astype(bf16)
    cross = mm(low, gates, 0, 0)
    up = cross[:RANK, :lanes]
    for p in range(1, PACK):
        up = up + cross[RANK * p : RANK * (p + 1), lanes * p : lanes * (p + 1)]
    share = RANK // blocks
    for i, part in enumerate(two_parts(up)):
        at = 4 * BLOCK + rows + i * share
        for n in range(blocks):
            goes_ref[n, at : at + share] = part[share * n : share * (n + 1)]
    for i, part in enumerate(two_parts(bias)):
        bias_ref[i : i + 1] = part


def prepare_kernel(head_ref, adj_ref, wide_ref, off_ref, ex_ref, going_ref, wu_ref, offs_ref, column_ref):
    seqs, local_len, _ = adj_ref.shape
    lanes = ADDRESS_WIDTH
    pieces = PAYLOAD_WIDTH // lanes
    for b in range(seqs):
        for h in range(HEADS):
            for i in range(pieces):
                going_ref[b * HEADS + h, local_len * i : local_len * (i + 1)] = adj_ref[
                    b, :, lanes * (h * pieces + i) : lanes * (h * pieces + i + 1)
                ]
    going_ref[:, pieces * local_len :] = jnp.zeros(
        (going_ref.shape[0], going_ref.shape[1] - pieces * local_len, lanes), bf16
    )
    at = pl.multiple_of(head_ref[0] * lanes, lanes)
    wu_ref[...] = wide_ref[:, pl.ds(at, lanes)]
    offs_ref[...] = off_ref[:, pl.ds(at, lanes)]
    blocks = column_ref.shape[1]
    row_id = lax.broadcasted_iota(jnp.int32, (BLOCK, BLOCK), 0)
    col_id = lax.broadcasted_iota(jnp.int32, (BLOCK, BLOCK), 1)
    place = lax.broadcasted_iota(jnp.int32, (BLOCK, blocks), 1)
    columns = jnp.zeros((BLOCK, blocks), f32)
    for n in range(blocks):
        row = ex_ref[:, BLOCK * n : BLOCK * (n + 1)]
        column = jnp.sum(jnp.where(row_id == col_id, row, 0.0), axis=1, keepdims=True)
        columns = jnp.where(place == n, column, columns)
    column_ref[...] = columns


def prepare(head, adj, wide, off, ex):
    seqs, local_len, _ = adj.shape
    rows = PAYLOAD_WIDTH // ADDRESS_WIDTH * local_len + BLOCK // PACK
    everything = pl.BlockSpec(memory_space=pltpu.VMEM)
    return pl.pallas_call(
        prepare_kernel,
        out_shape=(
            jax.ShapeDtypeStruct((seqs * HEADS, rows, ADDRESS_WIDTH), bf16),
            jax.ShapeDtypeStruct((RANK, ADDRESS_WIDTH), bf16),
            jax.ShapeDtypeStruct((1, ADDRESS_WIDTH), f32),
            jax.ShapeDtypeStruct((BLOCK, ex.shape[1] // BLOCK), f32),
        ),
        in_specs=[pl.BlockSpec(memory_space=pltpu.SMEM)] + [everything] * 4,
        name="prepare",
    )(head.astype(jnp.int32)[None], adj, wide, off, ex)


def mixer(came, wu, off, ex, q, k, v):
    blocks = q.shape[0]
    A, V = ADDRESS_WIDTH, PAYLOAD_WIDTH
    rows = BLOCK // PACK
    vmem = lambda shape, dt: pltpu.VMEM(shape, dt)
    return pl.pallas_call(
        mixer_kernel,
        out_shape=(
            jax.ShapeDtypeStruct((blocks, 4 * BLOCK + rows + 2 * RANK // blocks, A), bf16),
            jax.ShapeDtypeStruct((2, A), bf16),
        ),
        scratch_shapes=[
            vmem((A, PACK * A), bf16),
            vmem((6 * BLOCK, blocks * A), bf16),
            vmem((blocks, BLOCK, A), f32),
            vmem((blocks, BLOCK, A), f32),
            vmem((blocks, BLOCK, A), bf16),
            vmem((blocks, BLOCK, A), bf16),
            vmem((blocks, V, A), f32),
            vmem((blocks, BLOCK, BLOCK), bf16),
            vmem((blocks, BLOCK, A), f32),
            vmem((blocks, BLOCK, A), f32),
            vmem((blocks, BLOCK, A), f32),
            vmem((blocks, BLOCK, A), f32),
            vmem((blocks, 1, A), f32),
            vmem((blocks * rows, PACK * A), bf16),
        ],
        name="mixer",
    )(came, wu, off, ex, q, k, v)


def exchanged(tensor, axis):
    return lax.all_to_all(tensor, axis, split_axis=0, concat_axis=0, tiled=True)


def everyones(tensor, axis):
    return exchanged(jnp.broadcast_to(tensor, (lax.axis_size(axis), *tensor.shape)), axis)


def in_rows(tensor, lanes=128):
    flat = tensor.reshape(*tensor.shape[:-2], -1)
    pad = -flat.shape[-1] % lanes
    flat = jnp.pad(flat, [(0, 0)] * (flat.ndim - 1) + [(0, pad)])
    return flat.reshape(*flat.shape[:-1], -1, lanes)


def on_device(
    standardized_block_source,
    forgetting_narrowing_matrix,
    forgetting_widening_matrix,
    forgetting_offset_vector,
    probe_vectors,
    address_vectors,
    payload_vectors,
    extra_channel_forgetting,
    blender_result_adjoint,
):
    seqs, local_len, width = standardized_block_source.shape
    tokens = seqs * local_len
    length = probe_vectors.shape[1]
    blocks = length // BLOCK
    sp = lax.axis_size("sp")
    dp = lax.axis_size("dp")
    part = forgetting_narrowing_matrix.shape[0]
    A, V, R = ADDRESS_WIDTH, PAYLOAD_WIDTH, RANK
    rows = BLOCK // PACK
    contract = (((0,), (0,)), ((), ()))
    flat_input = standardized_block_source.reshape(tokens, width)

    down_rows = everyones(in_rows(forgetting_narrowing_matrix), "dp")
    down = down_rows.reshape(dp, -1)[:, : part * R].reshape(width, R)
    going, columns, offsets, extra = prepare(
        lax.axis_index("sp") % HEADS,
        blender_result_adjoint,
        forgetting_widening_matrix,
        forgetting_offset_vector[None],
        extra_channel_forgetting,
    )
    low = jnp.dot(flat_input, down, preferred_element_type=f32).astype(bf16)
    low = low.reshape(seqs, PACK, rows, R).transpose(0, 2, 1, 3).reshape(seqs, 1, rows, PACK * R)
    low = jnp.broadcast_to(low, (seqs, HEADS, rows, PACK * R)).reshape(sp, rows, A)
    going = lax.dynamic_update_slice(going, low, (0, 2 * BLOCK, 0))
    came = exchanged(going, "sp")
    goes, bias = mixer(
        came,
        columns,
        offsets,
        extra,
        probe_vectors.reshape(blocks, BLOCK, A),
        address_vectors.reshape(blocks, BLOCK, A),
        payload_vectors.reshape(blocks, BLOCK, V),
    )

    share = R // sp
    returned = exchanged(goes, "sp")
    first = returned[:, 4 * BLOCK :].astype(f32)
    low_grad = jnp.sum(first[:, :rows].reshape(seqs, HEADS, rows, A), axis=1).astype(bf16)
    low_grad = low_grad.reshape(seqs, rows, PACK, R).transpose(0, 2, 1, 3).reshape(tokens, R)
    up = first[:, rows : rows + share] + first[:, rows + share : rows + 2 * share]
    up = jnp.sum(up.reshape(seqs, HEADS * share, A), axis=0)

    def to_tokens(start, pieces):
        block = returned[:, start * BLOCK : (start + pieces) * BLOCK]
        block = block.reshape(seqs, HEADS, pieces, local_len, A)
        return block.transpose(0, 3, 1, 2, 4).reshape(seqs, local_len, HEADS * pieces * A)

    grad_input = jnp.dot(low_grad, down.T, preferred_element_type=f32).astype(bf16)
    whole = lax.dot_general(flat_input, low_grad, contract, preferred_element_type=f32)
    whole = in_rows(whole.astype(bf16).reshape(dp, part, R))
    n_whole = whole.shape[1]
    own = jnp.concatenate([up.astype(bf16), bias], axis=0)
    second = exchanged(
        jnp.concatenate([whole, jnp.broadcast_to(own, (dp, *own.shape))], axis=1), "dp"
    )
    second = jnp.sum(second.astype(f32), axis=0)
    second = jnp.concatenate(
        [second[:-2].astype(bf16), *two_parts(second[-2:-1] + second[-1:])], axis=0
    )
    third = everyones(second, "sp").astype(f32)
    down_grad = jnp.sum(third[:, :n_whole], axis=0).reshape(-1)[: part * R].reshape(part, R)
    up_grad = (
        third[:, n_whole:-2]
        .reshape(sp, HEADS, share, A)
        .transpose(0, 2, 1, 3)
        .reshape(R, HEADS * A)
    )
    bias_grad = jnp.sum((third[:, -2] + third[:, -1]).reshape(seqs, HEADS * A), axis=0)
    return (
        to_tokens(0, 1),
        to_tokens(1, 1),
        to_tokens(2, 2),
        grad_input.reshape(seqs, local_len, width),
        down_grad,
        up_grad,
        bias_grad,
    )


def solution(mesh):
    placed = (
        P("dp", "sp", None),
        P("dp", None),
        P(),
        P(),
        P(("dp", "sp"), None, None),
        P(("dp", "sp"), None, None),
        P(("dp", "sp"), None, None),
        P(("dp", "sp"), None),
        P("dp", "sp", None),
    )
    return jax.shard_map(
        on_device,
        mesh=mesh,
        in_specs=placed,
        out_specs=(
            P("dp", "sp", None),
            P("dp", "sp", None),
            P("dp", "sp", None),
            P("dp", "sp", None),
            P("dp", None),
            P(),
            P(),
        ),
        check_vma=False,
    )
```

time: 767 us -> 158 us (0.21)
  waiting for transfers between devices: 500 us -> 35.3 us
  local copies, waits for them, and re-layouts: 110 us -> 10.4 us
  matrix products: 65 us -> 0.96 us
  blocking collectives: 0 us -> 63.3 us
  other arithmetic: 30.7 us -> 1.76 us
  Pallas kernels: 0 us -> 15.9 us
  between operations: 14.4 us -> 0.93 us
  starting transfers between devices: 39 us -> 29.1 us
    psum x1 -> x0, waiting for transfers between devices: 449 us -> none  [in_one(): running = lax.psum(vector, axis)]
    dot_general x166 -> x3, matrix products: 65 us -> 0.96 us  [the longest x1 0.43 us: on_device(): jnp.dot(low_grad, down.T, preferred_element_type=f32).astype(bf16)]
    all_to_all x0 -> x2, blocking collectives: none -> 63.3 us  [exchanged(): return lax.all_to_all(tensor, axis, split_axis=0, concat_axis=0, tiled=True)]
    squeeze x96 -> x0, local copies, waits for them, and re-layouts: 38.5 us -> none  [the longest x64 38.4 us: head_forward(): lax.scan(jax.checkpoint(advance), initial, (blocked(scaled), blocked(stre...]
    dynamic_update_slice x16 -> x1, local copies, waits for them, and re-layouts: 27.9 us -> 0.01 us  [on_device(): going = lax.dynamic_update_slice(going, low, (0, 2 * BLOCK, 0))]
    dynamic_slice x33 -> x0, local copies, waits for them, and re-layouts: 16.1 us -> none  [the longest x32 16.1 us: head_forward(): lax.scan(jax.checkpoint(advance), initial, (blocked(scaled), blocked(stre...]
    pallas_call x0 -> x2, Pallas kernels: none -> 15.9 us  [the longest x1 13.3 us: mixer(): pl.pallas_call(mixer_kernel, out_shape=(jax.ShapeDtypeStruct((blocks, 4 *...]
    all_to_all x4 -> x3, waiting for transfers between devices: 50.8 us -> 35.3 us  [exchanged(): return lax.all_to_all(tensor, axis, split_axis=0, concat_axis=0, tiled=True)]
  transfers between devices with their start and end apart: 5 -> 3, of which waited for: 4 -> 3; matrix products, arithmetic and copies ran while one was open for 5% -> 3% of each run, Pallas kernels for 0% -> 2%
where the time goes in v1:
time: 158 us
  blocking collectives  63.3 us (40%)
  waiting for transfers between devices  35.3 us (22%)
  starting transfers between devices  29.1 us (18%)
  Pallas kernels  15.9 us (10%)
  local copies, waits for them, and re-layouts  10.4 us (7%)
  other arithmetic  1.76 us (1%)
    all_to_all x2, blocking collectives, exchanged(): return lax.all_to_all(tensor, axis, split_axis=0, concat_axis=0, tiled=True)  63.3 us
    all_to_all x3, waiting for transfers between devices, exchanged(): return lax.all_to_all(tensor, axis, split_axis=0, concat_axis=0, tiled=True)  35.3 us
    all_to_all x3, starting transfers between devices, exchanged(): return lax.all_to_all(tensor, axis, split_axis=0, concat_axis=0, tiled=True)  29.1 us
    pallas_call x1, Pallas kernels, mixer(): pl.pallas_call(mixer_kernel, out_shape=(jax.ShapeDtypeStruct((blocks, 4 *...  13.3 us
  transfers between devices with their start and end apart: 3, of which 3 were waited for; matrix products, arithmetic and copies ran while one was open for 3% of the time, Pallas kernels for 2%

profile of v1, /device:TPU:1, one launch (start us, length us, event | category | flops | bytes accessed | tf_op | source)
XLA Modules:
  0.0 157.6 jit_solution(18129247313593097005)
XLA Ops:
  0.6 0.0 copy-start
  0.6 0.8 copy.78
  1.5 0.1 reshape.96
  1.6 0.7 broadcast_in_dim.24
  2.3 18.8 %all-to-all-start = ((bf16[48,11,128]{2,1,0:T(8,128)(2,1)}), bf16[48,11,128]{2,1,0:T(8,128)(2,1)S(1)}, u32[]{:S(2)}, u32[]{:S(2)}) async-start(bf16[48,11,128]{2,1,0:T(8,128)(2,1)} %broadcast_in_dim.24), calls=%async_computation | async-start | bytes 393216 | tf_op jit(solution)/shard_map/all_to_all | solution.py:292
  21.2 2.6 %prepare.1 = (bf16[16,144,128]{2,1,0:T(8,128)(2,1)}, bf16[32,128]{1,0:T(8,128)(2,1)}, f32[1,128]{1,0:T(1,128)}, f32[64,16]{1,0:T(8,128)}) custom-call(s32[1]{0:T(128)} %bitcast.head_ref, bf16[2,64,2048]{2,1,0:T(8,128)(2,1)} %adj_ref.1, bf16[32,1024]{1,0:T(8,128)(2,1)} %wide_ref.1, f32[1,1024]{1,0:T(1,128)} %bitcast.84, f32[1,1024]{1,0:T(1,128)} %ex_ref.1), custom_call_target="tpu_custom_call" | custom-call | tf_op jit(solution)/shard_map/prepare/pallas_call | solution.py:247
  23.7 11.4 %all-to-all-done = bf16[48,11,128]{2,1,0:T(8,128)(2,1)S(1)} async-done(((bf16[48,11,128]{2,1,0:T(8,128)(2,1)}), bf16[48,11,128]{2,1,0:T(8,128)(2,1)S(1)}, u32[]{:S(2)}, u32[]{:S(2)}) %all-to-all-start) | async-done | bytes 135200 | tf_op jit(solution)/shard_map/all_to_all | solution.py:292
  35.1 0.0 copy-start.1
  35.1 0.5 reshape.99
  35.6 0.0 copy-done
  35.6 0.3 fusion.1
  35.9 0.1 copy.79
  36.1 0.1 broadcast_in_dim.25
  36.2 0.0 copy-done.1
  36.2 28.8 %all_to_all.25.came_ref = bf16[16,144,128]{2,1,0:T(8,128)(2,1)} all-to-all(bf16[16,144,128]{2,1,0:T(8,128)(2,1)S(1)} %constant_dynamic-update-slice_fusion), channel_id=1, replica_groups=mesh['sp'=16,'dp'=48] {'sp'}, dimensions={0} | all-to-all | bytes 1179648 | tf_op jit(solution)/shard_map/all_to_all | solution.py:292
  65.0 13.3 %mixer.1 = (bf16[16,276,128]{2,1,0:T(8,128)(2,1)}, bf16[2,128]{1,0:T(2,128)(2,1)}) custom-call(bf16[16,144,128]{2,1,0:T(8,128)(2,1)} %all_to_all.25.came_ref, bf16[32,128]{1,0:T(8,128)(2,1)} %get-tuple-element.14.wu_ref, f32[1,128]{1,0:T(1,128)} %get-tuple-element.15.off_ref, f32[64,16]{1,0:T(8,128)} %get-tuple-element.16.ex_ref, ...), custom_call_target="tpu_custom_call" | custom-call | tf_op jit(solution)/shard_map/mixer/pallas_call | solution.py:265
  78.3 34.6 %all_to_all.26 = bf16[16,276,128]{2,1,0:T(8,128)(2,1)S(1)} all-to-all(bf16[16,276,128]{2,1,0:T(8,128)(2,1)} %get-tuple-element.17), channel_id=1, replica_groups=mesh['sp'=16,'dp'=48] {'sp'}, dimensions={0} | all-to-all | bytes 2260992 | tf_op jit(solution)/shard_map/all_to_all | solution.py:292
  112.9 0.1 convert_element_type.52
  113.0 0.2 fusion
  113.3 0.0 copy-start.2
  113.3 0.3 copy.86
  113.6 0.3 reshape_reshape.3
  113.9 0.1 reshape.115
  114.0 0.0 copy-done.2
  114.1 0.9 pad_maximum_fusion
  115.0 4.5 %all-to-all-start.3 = ((bf16[48,29,128]{2,1,0:T(8,128)(2,1)}), bf16[48,29,128]{2,1,0:T(8,128)(2,1)S(1)}, u32[]{:S(2)}, u32[]{:S(2)}) async-start(bf16[48,29,128]{2,1,0:T(8,128)(2,1)} %pad_maximum_fusion), calls=%async_computation.3 | async-start | bytes 786432 | tf_op jit(solution)/shard_map/all_to_all | solution.py:292
  119.5 0.4 convolution_convert_fusion
  119.9 1.1 copy.85
  121.0 18.6 %all-to-all-done.3 = bf16[48,29,128]{2,1,0:T(8,128)(2,1)S(1)} async-done(((bf16[48,29,128]{2,1,0:T(8,128)(2,1)}), bf16[48,29,128]{2,1,0:T(8,128)(2,1)S(1)}, u32[]{:S(2)}, u32[]{:S(2)}) %all-to-all-start.3) | async-done | bytes 356384 | tf_op jit(solution)/shard_map/all_to_all | solution.py:292
  139.6 0.1 convert_reduce_fusion
  139.8 0.7 broadcast_in_dim.28
  140.4 5.7 %all-to-all-start.4 = ((bf16[16,29,128]{2,1,0:T(8,128)(2,1)}), bf16[16,29,128]{2,1,0:T(8,128)(2,1)S(1)}, u32[]{:S(2)}, u32[]{:S(2)}) async-start(bf16[16,29,128]{2,1,0:T(8,128)(2,1)} %broadcast_in_dim.28), calls=%async_computation.4 | async-start | bytes 262144 | tf_op jit(solution)/shard_map/all_to_all | solution.py:292
  146.2 0.2 copy.82
  146.3 0.8 reshape.109
  147.2 0.2 copy.81
  147.3 0.8 reshape.107
  148.2 0.5 copy.83
  148.8 1.2 reshape.111
  149.9 5.4 %all-to-all-done.4 = bf16[16,29,128]{2,1,0:T(8,128)(2,1)S(1)} async-done(((bf16[16,29,128]{2,1,0:T(8,128)(2,1)}), bf16[16,29,128]{2,1,0:T(8,128)(2,1)S(1)}, u32[]{:S(2)}, u32[]{:S(2)}) %all-to-all-start.4) | async-done | bytes 118816 | tf_op jit(solution)/shard_map/all_to_all | solution.py:292
  155.4 0.1 copy.89
  155.5 0.7 copy.98
  156.2 0.1 slice.64
  156.3 0.7 copy.90
  157.0 0.6 reduce_sum.49
  (23 shorter events, 0.4 us)
Async XLA Ops:
  0.6 35.0 %copy-start = (bf16[2,64,2064]{2,1,0:T(8,128)(2,1)S(1)}, bf16[2,64,2064]{2,1,0:T(8,128)(2,1)}, u32[]{:S(2)}) copy-start(bf16[2,64,2064]{2,1,0:T(8,128)(2,1)} %param.9) | copy-start | bytes 1585156
  2.3 32.8 %all-to-all-start = ((bf16[48,11,128]{2,1,0:T(8,128)(2,1)}), bf16[48,11,128]{2,1,0:T(8,128)(2,1)S(1)}, u32[]{:S(2)}, u32[]{:S(2)}) async-start(bf16[48,11,128]{2,1,0:T(8,128)(2,1)} %broadcast_in_dim.24), calls=%async_computation | async-start | bytes 393216 | tf_op jit(solution)/shard_map/all_to_all | solution.py:292
  35.1 1.1 copy-start.1
  113.3 0.7 copy-start.2
  115.0 24.6 %all-to-all-start.3 = ((bf16[48,29,128]{2,1,0:T(8,128)(2,1)}), bf16[48,29,128]{2,1,0:T(8,128)(2,1)S(1)}, u32[]{:S(2)}, u32[]{:S(2)}) async-start(bf16[48,29,128]{2,1,0:T(8,128)(2,1)} %pad_maximum_fusion), calls=%async_computation.3 | async-start | bytes 786432 | tf_op jit(solution)/shard_map/all_to_all | solution.py:292
  140.4 14.9 %all-to-all-start.4 = ((bf16[16,29,128]{2,1,0:T(8,128)(2,1)}), bf16[16,29,128]{2,1,0:T(8,128)(2,1)S(1)}, u32[]{:S(2)}, u32[]{:S(2)}) async-start(bf16[16,29,128]{2,1,0:T(8,128)(2,1)} %broadcast_in_dim.28), calls=%async_computation.4 | async-start | bytes 262144 | tf_op jit(solution)/shard_map/all_to_all | solution.py:292

commit v2 on v1

--- a/solution.py
+++ b/solution.py
@@ -13,6 +13,8 @@
 SMOOTHING = 16.0
 SPAN_LIMIT = 80.0
 PACK = 4
+GROUP = 4
+UNROLL = 4
 f32 = jnp.float32
 bf16 = jnp.bfloat16
 
@@ -32,19 +34,36 @@
 
 
 def mixer_kernel(
-    came_ref, wu_ref, off_ref, ex_ref, q_ref, k_ref, v_ref,
-    goes_ref, bias_ref,
-    wbig, parts, b_s, pre_s, qp_s, kf_s, st_s, pt_s, dqi_s, dki_s, x_s, y_s, e_s, gate_s,
+    came_hbm, wu_ref, off_ref, ex_ref, q_hbm, k_hbm, v_hbm,
+    goes_hbm, bias_ref,
+    low_s, do_ref, q_ref, k_ref, v_ref, goes_ref, wbig, parts, b_s, pre_s, qp_s, kf_s, st_s,
+    pt_s, dqi_s, dki_s, x_s, y_s, e_s, gate_s, sems,
 ):
     blocks = q_ref.shape[0]
     rows = BLOCK // PACK
     lanes = ADDRESS_WIDTH
     scale = ADDRESS_WIDTH ** (-0.5)
     middle = BLOCK // 2
-
-    def do_block(n):
+    group = GROUP * BLOCK
+    halves = PAYLOAD_WIDTH // lanes
+
+    copies = [
+        pltpu.make_async_copy(came_hbm.at[:, halves * BLOCK :], low_s, sems.at[0]),
+        pltpu.make_async_copy(q_hbm, q_ref, sems.at[1]),
+        pltpu.make_async_copy(k_hbm, k_ref, sems.at[2]),
+        pltpu.make_async_copy(came_hbm.at[:, : halves * BLOCK], do_ref, sems.at[3]),
+        pltpu.make_async_copy(v_hbm, v_ref, sems.at[4]),
+    ]
+    for copy in copies:
+        copy.start()
+
+    def do_rows(at, count):
+        both = do_ref[pl.ds(at, count)]
         return jnp.concatenate(
-            [came_ref[n, BLOCK * i : BLOCK * (i + 1)] for i in range(PAYLOAD_WIDTH // lanes)],
+            [
+                both[:, BLOCK * i : BLOCK * (i + 1)].reshape(count * BLOCK, lanes)
+                for i in range(halves)
+            ],
             axis=1,
         )
 
@@ -54,7 +73,8 @@
     wbig[...] = jnp.zeros(wbig.shape, bf16)
     for p in range(PACK):
         wbig[RANK * p : RANK * (p + 1), lanes * p : lanes * (p + 1)] = wu_ref[...]
-    low = came_ref[:, 2 * BLOCK :].reshape(blocks * rows, lanes)
+    copies[0].wait()
+    low = low_s[...].reshape(blocks * rows, lanes)
     raw = mm(low, wbig[...])
     offs = off_ref[...]
     for n in range(blocks):
@@ -83,97 +103,151 @@
         centre = b[middle : middle + 1]
         span = jnp.maximum(span, jnp.maximum(b[:1] - centre, centre - b[BLOCK - 1 :]))
     narrow = jnp.max(span) < SPAN_LIMIT
+    for copy in copies[1:]:
+        copy.wait()
 
     @pl.when(narrow)
     def _():
-        def within(n, carry):
-            b = b_s[n]
-            centre = b[middle : middle + 1]
-            lift = jnp.exp(b - centre)
-            drop = jnp.exp(centre - b)
-            qc = (q_ref[n].astype(f32) * scale * lift).astype(bf16)
-            kc = (k_ref[n].astype(f32) * drop).astype(bf16)
-            do = do_block(n)
-            v = v_ref[n]
-            pt_s[n] = jnp.where(row_id <= col_id, mm(kc, qc, 1, 1), 0.0).astype(bf16)
-            dp = jnp.where(row_id >= col_id, mm(do, v, 1, 1), 0.0).astype(bf16)
+        big_row = lax.broadcasted_iota(jnp.int32, (group, group), 0)
+        big_col = lax.broadcasted_iota(jnp.int32, (group, group), 1)
+        same = big_row // BLOCK == big_col // BLOCK
+        causal = same & (big_row >= big_col)
+        mirrored = same & (big_row <= big_col)
+
+        def within(g, carry):
+            at = g * GROUP
+            b = b_s[pl.ds(at, GROUP)]
+            centre = b[:, middle : middle + 1]
+            lift = jnp.exp(b - centre).reshape(group, lanes)
+            drop = jnp.exp(centre - b).reshape(group, lanes)
+            q = q_ref[pl.ds(at, GROUP)].astype(f32).reshape(group, lanes)
+            k = k_ref[pl.ds(at, GROUP)].astype(f32).reshape(group, lanes)
+            qc = (q * scale * lift).astype(bf16)
+            kc = (k * drop).astype(bf16)
+            do = do_rows(at, GROUP)
+            v = v_ref[pl.ds(at, GROUP)].reshape(group, PAYLOAD_WIDTH)
+            pt_s[g] = jnp.where(mirrored, mm(kc, qc, 1, 1), 0.0).astype(bf16)
+            dp = jnp.where(causal, mm(do, v, 1, 1), 0.0).astype(bf16)
             dq = mm(dp, kc)
             dk = mm(dp, qc, 0, 0)
-            x_s[n] = dq * qc.astype(f32) - dk * kc.astype(f32)
-            dqi_s[n] = dq * lift
-            dki_s[n] = dk * drop
+            shape = (GROUP, BLOCK, lanes)
+            x_s[pl.ds(at, GROUP)] = (dq * qc.astype(f32) - dk * kc.astype(f32)).reshape(shape)
+            dqi_s[pl.ds(at, GROUP)] = (dq * lift).reshape(shape)
+            dki_s[pl.ds(at, GROUP)] = (dk * drop).reshape(shape)
             return carry
 
-        lax.fori_loop(0, blocks, within, 0, unroll=4)
+        lax.fori_loop(0, blocks // GROUP, within, 0, unroll=UNROLL)
 
     @pl.when(jnp.logical_not(narrow))
     def _():
-        def within(n, carry):
-            b = b_s[n]
-            q = q_ref[n].astype(f32) * scale
-            dp = mm(do_block(n), v_ref[n], 1, 1)
-            at = lax.broadcasted_iota(jnp.int32, (BLOCK, 1), 0)
-            dqi_s[n] = jnp.zeros((BLOCK, lanes), f32)
-            x_s[n] = jnp.zeros((BLOCK, lanes), f32)
-
-            def one(s, scores):
-                here = at == s
-                b_row = jnp.sum(jnp.where(here, b, 0.0), axis=0, keepdims=True)
-                k_row = jnp.sum(
-                    jnp.where(here, k_ref[n].astype(f32), 0.0), axis=0, keepdims=True
+        pt_s[...] = jnp.zeros(pt_s.shape, bf16)
+        for m in range(GROUP):
+            def within(g, carry, m=m):
+                n = g * GROUP + m
+                b = b_s[n]
+                q = q_ref[n].astype(f32) * scale
+                dp = mm(do_rows(n, 1), v_ref[n], 1, 1)
+                at = lax.broadcasted_iota(jnp.int32, (BLOCK, 1), 0)
+                dqi_s[n] = jnp.zeros((BLOCK, lanes), f32)
+                x_s[n] = jnp.zeros((BLOCK, lanes), f32)
+
+                def one(s, scores):
+                    here = at == s
+                    b_row = jnp.sum(jnp.where(here, b, 0.0), axis=0, keepdims=True)
+                    k_row = jnp.sum(
+                        jnp.where(here, k_ref[n].astype(f32), 0.0), axis=0, keepdims=True
+                    )
+                    decay = jnp.where(at >= s, jnp.exp(jnp.minimum(b - b_row, 0.0)), 0.0)
+                    dp_col = jnp.sum(jnp.where(col_id == s, dp, 0.0), axis=1, keepdims=True)
+                    qd = q * decay
+                    column = jnp.sum(qd * k_row, axis=1, keepdims=True)
+                    dq = dp_col * decay * k_row
+                    dk_row = jnp.sum(dp_col * qd, axis=0, keepdims=True)
+                    dqi_s[n] = dqi_s[n] + dq
+                    dki_s[n] = jnp.where(here, dk_row, dki_s[n])
+                    x_s[n] = x_s[n] + q * dq - jnp.where(here, dk_row * k_row, 0.0)
+                    return scores + jnp.where(col_id == s, column, 0.0)
+
+                scores = lax.fori_loop(0, BLOCK, one, jnp.zeros((BLOCK, BLOCK), f32))
+                pt_s[g, BLOCK * m : BLOCK * (m + 1), BLOCK * m : BLOCK * (m + 1)] = (
+                    scores.T.astype(bf16)
                 )
-                decay = jnp.where(at >= s, jnp.exp(jnp.minimum(b - b_row, 0.0)), 0.0)
-                dp_col = jnp.sum(jnp.where(col_id == s, dp, 0.0), axis=1, keepdims=True)
-                qd = q * decay
-                column = jnp.sum(qd * k_row, axis=1, keepdims=True)
-                dq = dp_col * decay * k_row
-                dk_row = jnp.sum(dp_col * qd, axis=0, keepdims=True)
-                dqi_s[n] = dqi_s[n] + dq
-                dki_s[n] = jnp.where(here, dk_row, dki_s[n])
-                x_s[n] = x_s[n] + q * dq - jnp.where(here, dk_row * k_row, 0.0)
-                return scores + jnp.where(col_id == s, column, 0.0)
-
-            scores = lax.fori_loop(0, BLOCK, one, jnp.zeros((BLOCK, BLOCK), f32))
-            pt_s[n] = scores.T.astype(bf16)
-            return carry
-
-        lax.fori_loop(0, blocks, within, 0)
-
-    def forward(n, state):
-        b = b_s[n]
-        last = b[BLOCK - 1 :]
+                return carry
+
+            lax.fori_loop(0, blocks // GROUP, within, 0)
+
+    def spread(tensor):
+        zero = jnp.zeros((BLOCK, lanes), tensor.dtype)
+        return jnp.concatenate(
+            [
+                jnp.concatenate(
+                    [tensor[m] if m == i else zero for i in range(GROUP)], axis=0
+                )
+                for m in range(GROUP)
+            ],
+            axis=1,
+        )
+
+    def forward(g, state):
+        at = g * GROUP
+        b = b_s[pl.ds(at, GROUP)]
+        last = b[:, BLOCK - 1 :]
         grow = jnp.exp(b)
-        qp = (q_ref[n].astype(f32) * scale * grow).astype(bf16)
-        kf = (k_ref[n].astype(f32) * jnp.exp(last - b)).astype(bf16)
-        qp_s[n] = qp
-        kf_s[n] = kf
-        st_s[n] = state
-        dq = mm(do_block(n), state.astype(bf16))
-        x_s[n] = x_s[n] + qp.astype(f32) * dq
-        goes_ref[n, :BLOCK] = ((dqi_s[n] + dq * grow) * scale).astype(bf16)
-        return state * jnp.exp(last) + mm(v_ref[n], kf, 0, 0)
+        fade = jnp.exp(last)
+        qp = (q_ref[pl.ds(at, GROUP)].astype(f32) * scale * grow).astype(bf16)
+        kf = (k_ref[pl.ds(at, GROUP)].astype(f32) * jnp.exp(last - b)).astype(bf16)
+        qp_s[pl.ds(at, GROUP)] = qp
+        kf_s[pl.ds(at, GROUP)] = kf
+        v = v_ref[pl.ds(at, GROUP)].reshape(group, PAYLOAD_WIDTH)
+        added = mm(v, spread(kf), 0, 0)
+        do = do_rows(at, GROUP)
+        for m in range(GROUP):
+            n = at + m
+            st_s[n] = state
+            dq = mm(do[BLOCK * m : BLOCK * (m + 1)], state.astype(bf16))
+            x_s[n] = x_s[n] + qp[m].astype(f32) * dq
+            goes_ref[n, :BLOCK] = ((dqi_s[n] + dq * grow[m]) * scale).astype(bf16)
+            state = state * fade[m] + added[:, lanes * m : lanes * (m + 1)]
+        return state
 
     zero = jnp.zeros((PAYLOAD_WIDTH, lanes), f32)
-    lax.fori_loop(0, blocks, forward, zero, unroll=4)
+    lax.fori_loop(0, blocks // GROUP, forward, zero, unroll=UNROLL)
+    out_q = pltpu.make_async_copy(
+        goes_ref.at[:, :BLOCK], goes_hbm.at[:, :BLOCK], sems.at[5]
+    )
+    out_q.start()
 
     def backward(i, dstate):
-        n = blocks - 1 - i
-        b = b_s[n]
-        last = b[BLOCK - 1 :]
-        do = do_block(n)
-        ds = dstate.astype(bf16)
-        kf = kf_s[n]
-        dk = mm(v_ref[n], ds)
-        goes_ref[n, BLOCK : 2 * BLOCK] = (dki_s[n] + dk * jnp.exp(last - b)).astype(bf16)
-        dv = (mm(pt_s[n], do) + mm(kf, ds, 1, 1)).astype(bf16)
-        goes_ref[n, 2 * BLOCK : 3 * BLOCK] = dv[:, :lanes]
-        goes_ref[n, 3 * BLOCK : 4 * BLOCK] = dv[:, lanes:]
-        y_s[n] = kf.astype(f32) * dk
+        g = blocks // GROUP - 1 - i
+        at = g * GROUP
+        b = b_s[pl.ds(at, GROUP)]
+        last = b[:, BLOCK - 1 :]
+        drop = jnp.exp(last - b)
         fade = jnp.exp(last)
-        e_s[n] = fade * jnp.sum(st_s[n] * dstate, axis=0, keepdims=True)
-        return dstate * fade + mm(do, qp_s[n], 0, 0)
-
-    lax.fori_loop(0, blocks, backward, zero, unroll=4)
+        do = do_rows(at, GROUP)
+        added = mm(do, spread(qp_s[pl.ds(at, GROUP)]), 0, 0)
+        dv_own = mm(pt_s[g], do)
+        for m in reversed(range(GROUP)):
+            n = at + m
+            ds = dstate.astype(bf16)
+            kf = kf_s[n]
+            dk = mm(v_ref[n], ds)
+            goes_ref[n, BLOCK : 2 * BLOCK] = (dki_s[n] + dk * drop[m]).astype(bf16)
+            dv = (dv_own[BLOCK * m : BLOCK * (m + 1)] + mm(kf, ds, 1, 1)).astype(bf16)
+            for i in range(halves):
+                goes_ref[n, BLOCK * (2 + i) : BLOCK * (3 + i)] = dv[
+                    :, lanes * i : lanes * (i + 1)
+                ]
+            y_s[n] = kf.astype(f32) * dk
+            e_s[n] = fade[m] * jnp.sum(st_s[n] * dstate, axis=0, keepdims=True)
+            dstate = dstate * fade[m] + added[:, lanes * m : lanes * (m + 1)]
+        return dstate
+
+    lax.fori_loop(0, blocks // GROUP, backward, zero, unroll=UNROLL)
+    out_kv = pltpu.make_async_copy(
+        goes_ref.at[:, BLOCK : 4 * BLOCK], goes_hbm.at[:, BLOCK : 4 * BLOCK], sems.at[6]
+    )
+    out_kv.start()
 
     for n in range(blocks):
         for i, part in enumerate(three_parts(x_s[n])):
@@ -198,18 +272,26 @@
             ]
     gates = gate_s[...]
     lowg = mm(gates, wbig[...], 1, 1)
-    goes_ref[:, 4 * BLOCK : 4 * BLOCK + rows] = lowg.reshape(blocks, rows, lanes).astype(bf16)
+    first = 4 * BLOCK
+    goes_ref[:, first : first + rows] = lowg.reshape(blocks, rows, lanes).astype(bf16)
     cross = mm(low, gates, 0, 0)
     up = cross[:RANK, :lanes]
     for p in range(1, PACK):
         up = up + cross[RANK * p : RANK * (p + 1), lanes * p : lanes * (p + 1)]
     share = RANK // blocks
     for i, part in enumerate(two_parts(up)):
-        at = 4 * BLOCK + rows + i * share
+        at = first + rows + i * share
         for n in range(blocks):
             goes_ref[n, at : at + share] = part[share * n : share * (n + 1)]
     for i, part in enumerate(two_parts(bias)):
         bias_ref[i : i + 1] = part
+    out_rest = pltpu.make_async_copy(
+        goes_ref.at[:, first:], goes_hbm.at[:, first:], sems.at[7]
+    )
+    out_rest.start()
+    out_q.wait()
+    out_kv.wait()
+    out_rest.wait()
 
 
 def prepare_kernel(head_ref, adj_ref, wide_ref, off_ref, ex_ref, going_ref, wu_ref, offs_ref, column_ref):
@@ -261,14 +343,25 @@
     blocks = q.shape[0]
     A, V = ADDRESS_WIDTH, PAYLOAD_WIDTH
     rows = BLOCK // PACK
-    vmem = lambda shape, dt: pltpu.VMEM(shape, dt)
+    height = 4 * BLOCK + rows + 2 * RANK // blocks
+    vmem = pltpu.VMEM
+    anywhere = pl.BlockSpec(memory_space=pl.ANY)
+    inside = pl.BlockSpec(memory_space=pltpu.VMEM)
     return pl.pallas_call(
         mixer_kernel,
         out_shape=(
-            jax.ShapeDtypeStruct((blocks, 4 * BLOCK + rows + 2 * RANK // blocks, A), bf16),
+            jax.ShapeDtypeStruct((blocks, height, A), bf16),
             jax.ShapeDtypeStruct((2, A), bf16),
         ),
+        in_specs=[anywhere, inside, inside, inside, anywhere, anywhere, anywhere],
+        out_specs=[anywhere, inside],
         scratch_shapes=[
+            vmem((blocks, rows, A), bf16),
+            vmem((blocks, V // A * BLOCK, A), bf16),
+            vmem((blocks, BLOCK, A), bf16),
+            vmem((blocks, BLOCK, A), bf16),
+            vmem((blocks, BLOCK, V), bf16),
+            vmem((blocks, height, A), bf16),
             vmem((A, PACK * A), bf16),
             vmem((6 * BLOCK, blocks * A), bf16),
             vmem((blocks, BLOCK, A), f32),
@@ -276,13 +369,14 @@
             vmem((blocks, BLOCK, A), bf16),
             vmem((blocks, BLOCK, A), bf16),
             vmem((blocks, V, A), f32),
-            vmem((blocks, BLOCK, BLOCK), bf16),
+            vmem((blocks // GROUP, GROUP * BLOCK, GROUP * BLOCK), bf16),
             vmem((blocks, BLOCK, A), f32),
             vmem((blocks, BLOCK, A), f32),
             vmem((blocks, BLOCK, A), f32),
             vmem((blocks, BLOCK, A), f32),
             vmem((blocks, 1, A), f32),
             vmem((blocks * rows, PACK * A), bf16),
+            pltpu.SemaphoreType.DMA((8,)),
         ],
         name="mixer",
     )(came, wu, off, ex, q, k, v)

time: 158 us -> 153 us (0.968)
  Pallas kernels: 15.9 us -> 10.7 us
    pallas_call x1, Pallas kernels: 13.3 us -> 8.17 us  [mixer(): pl.pallas_call(mixer_kernel, out_shape=(jax.ShapeDtypeStruct((blocks, hei...]
where the time goes in v2:
time: 153 us; the launch traced here: 152 us
  blocking collectives  63.3 us (41%)
  waiting for transfers between devices  35.3 us (23%)
  starting transfers between devices  29.1 us (19%)
  Pallas kernels  10.7 us (7%)
  local copies, waits for them, and re-layouts  10.4 us (7%)
  other arithmetic  1.76 us (1%)
    all_to_all x2, blocking collectives, exchanged(): return lax.all_to_all(tensor, axis, split_axis=0, concat_axis=0, tiled=True)  63.3 us
    all_to_all x3, waiting for transfers between devices, exchanged(): return lax.all_to_all(tensor, axis, split_axis=0, concat_axis=0, tiled=True)  35.3 us
    all_to_all x3, starting transfers between devices, exchanged(): return lax.all_to_all(tensor, axis, split_axis=0, concat_axis=0, tiled=True)  29.1 us
    pallas_call x1, Pallas kernels, mixer(): pl.pallas_call(mixer_kernel, out_shape=(jax.ShapeDtypeStruct((blocks, hei...  8.17 us
  transfers between devices with their start and end apart: 3, of which 3 were waited for; matrix products, arithmetic and copies ran while one was open for 3% of the time, Pallas kernels for 2%

profile of v2, /device:TPU:1, one launch (start us, length us, event | category | flops | bytes accessed | tf_op | source)
XLA Modules:
  0.0 152.5 jit_solution(10560575672997296344)
XLA Ops:
  0.6 0.0 copy-start
  0.6 0.8 copy.78
  1.5 0.1 reshape.96
  1.6 0.7 broadcast_in_dim.24
  2.3 18.8 %all-to-all-start = ((bf16[48,11,128]{2,1,0:T(8,128)(2,1)}), bf16[48,11,128]{2,1,0:T(8,128)(2,1)S(1)}, u32[]{:S(2)}, u32[]{:S(2)}) async-start(bf16[48,11,128]{2,1,0:T(8,128)(2,1)} %broadcast_in_dim.24), calls=%async_computation | async-start | bytes 393216 | tf_op jit(solution)/shard_map/all_to_all | solution.py:386
  21.2 2.6 %prepare.1 = (bf16[16,144,128]{2,1,0:T(8,128)(2,1)}, bf16[32,128]{1,0:T(8,128)(2,1)}, f32[1,128]{1,0:T(1,128)}, f32[64,16]{1,0:T(8,128)}) custom-call(s32[1]{0:T(128)} %bitcast.head_ref, bf16[2,64,2048]{2,1,0:T(8,128)(2,1)} %adj_ref.1, bf16[32,1024]{1,0:T(8,128)(2,1)} %wide_ref.1, f32[1,1024]{1,0:T(1,128)} %bitcast.84, f32[1,1024]{1,0:T(1,128)} %ex_ref.1), custom_call_target="tpu_custom_call" | custom-call | tf_op jit(solution)/shard_map/prepare/pallas_call | solution.py:329
  23.7 11.4 %all-to-all-done = bf16[48,11,128]{2,1,0:T(8,128)(2,1)S(1)} async-done(((bf16[48,11,128]{2,1,0:T(8,128)(2,1)}), bf16[48,11,128]{2,1,0:T(8,128)(2,1)S(1)}, u32[]{:S(2)}, u32[]{:S(2)}) %all-to-all-start) | async-done | bytes 135200 | tf_op jit(solution)/shard_map/all_to_all | solution.py:386
  35.1 0.0 copy-start.1
  35.1 0.5 reshape.99
  35.6 0.0 copy-done
  35.6 0.3 fusion.1
  35.9 0.1 copy.79
  36.1 0.1 broadcast_in_dim.25
  36.2 0.0 copy-done.1
  36.2 28.8 %all_to_all.25.came_hbm = bf16[16,144,128]{2,1,0:T(8,128)(2,1)} all-to-all(bf16[16,144,128]{2,1,0:T(8,128)(2,1)S(1)} %constant_dynamic-update-slice_fusion), channel_id=1, replica_groups=mesh['sp'=16,'dp'=48] {'sp'}, dimensions={0} | all-to-all | bytes 1179648 | tf_op jit(solution)/shard_map/all_to_all | solution.py:386
  65.0 8.2 %mixer.1 = (bf16[16,276,128]{2,1,0:T(8,128)(2,1)}, bf16[2,128]{1,0:T(2,128)(2,1)}) custom-call(bf16[16,144,128]{2,1,0:T(8,128)(2,1)} %all_to_all.25.came_hbm, bf16[32,128]{1,0:T(8,128)(2,1)} %get-tuple-element.14.wu_ref, f32[1,128]{1,0:T(1,128)} %get-tuple-element.15.off_ref, f32[64,16]{1,0:T(8,128)} %get-tuple-element.16.ex_ref, ...), custom_call_target="tpu_custom_call" | custom-call | tf_op jit(solution)/shard_map/mixer/pallas_call | solution.py:350
  73.2 34.6 %all_to_all.26 = bf16[16,276,128]{2,1,0:T(8,128)(2,1)S(1)} all-to-all(bf16[16,276,128]{2,1,0:T(8,128)(2,1)} %get-tuple-element.17), channel_id=1, replica_groups=mesh['sp'=16,'dp'=48] {'sp'}, dimensions={0} | all-to-all | bytes 2260992 | tf_op jit(solution)/shard_map/all_to_all | solution.py:386
  107.8 0.1 convert_element_type.52
  107.9 0.2 fusion
  108.1 0.0 copy-start.2
  108.2 0.3 copy.86
  108.5 0.3 reshape_reshape.3
  108.8 0.1 reshape.115
  108.9 0.0 copy-done.2
  109.0 0.9 pad_maximum_fusion
  109.8 4.5 %all-to-all-start.3 = ((bf16[48,29,128]{2,1,0:T(8,128)(2,1)}), bf16[48,29,128]{2,1,0:T(8,128)(2,1)S(1)}, u32[]{:S(2)}, u32[]{:S(2)}) async-start(bf16[48,29,128]{2,1,0:T(8,128)(2,1)} %pad_maximum_fusion), calls=%async_computation.3 | async-start | bytes 786432 | tf_op jit(solution)/shard_map/all_to_all | solution.py:386
  114.4 0.4 convolution_convert_fusion
  114.8 1.1 copy.85
  115.9 18.6 %all-to-all-done.3 = bf16[48,29,128]{2,1,0:T(8,128)(2,1)S(1)} async-done(((bf16[48,29,128]{2,1,0:T(8,128)(2,1)}), bf16[48,29,128]{2,1,0:T(8,128)(2,1)S(1)}, u32[]{:S(2)}, u32[]{:S(2)}) %all-to-all-start.3) | async-done | bytes 356384 | tf_op jit(solution)/shard_map/all_to_all | solution.py:386
  134.5 0.1 convert_reduce_fusion
  134.6 0.7 broadcast_in_dim.28
  135.3 5.7 %all-to-all-start.4 = ((bf16[16,29,128]{2,1,0:T(8,128)(2,1)}), bf16[16,29,128]{2,1,0:T(8,128)(2,1)S(1)}, u32[]{:S(2)}, u32[]{:S(2)}) async-start(bf16[16,29,128]{2,1,0:T(8,128)(2,1)} %broadcast_in_dim.28), calls=%async_computation.4 | async-start | bytes 262144 | tf_op jit(solution)/shard_map/all_to_all | solution.py:386
  141.1 0.2 copy.82
  141.2 0.8 reshape.109
  142.1 0.2 copy.81
  142.2 0.8 reshape.107
  143.1 0.5 copy.83
  143.7 1.2 reshape.111
  144.8 5.4 %all-to-all-done.4 = bf16[16,29,128]{2,1,0:T(8,128)(2,1)S(1)} async-done(((bf16[16,29,128]{2,1,0:T(8,128)(2,1)}), bf16[16,29,128]{2,1,0:T(8,128)(2,1)S(1)}, u32[]{:S(2)}, u32[]{:S(2)}) %all-to-all-start.4) | async-done | bytes 118816 | tf_op jit(solution)/shard_map/all_to_all | solution.py:386
  150.3 0.1 copy.89
  150.4 0.7 copy.98
  151.1 0.1 slice.64
  151.2 0.7 copy.90
  151.9 0.6 reduce_sum.49
  (23 shorter events, 0.4 us)
Async XLA Ops:
  0.6 35.0 %copy-start = (bf16[2,64,2064]{2,1,0:T(8,128)(2,1)S(1)}, bf16[2,64,2064]{2,1,0:T(8,128)(2,1)}, u32[]{:S(2)}) copy-start(bf16[2,64,2064]{2,1,0:T(8,128)(2,1)} %param.9) | copy-start | bytes 1585156
  2.3 32.8 %all-to-all-start = ((bf16[48,11,128]{2,1,0:T(8,128)(2,1)}), bf16[48,11,128]{2,1,0:T(8,128)(2,1)S(1)}, u32[]{:S(2)}, u32[]{:S(2)}) async-start(bf16[48,11,128]{2,1,0:T(8,128)(2,1)} %broadcast_in_dim.24), calls=%async_computation | async-start | bytes 393216 | tf_op jit(solution)/shard_map/all_to_all | solution.py:386
  35.1 1.1 copy-start.1
  108.1 0.7 copy-start.2
  109.8 24.6 %all-to-all-start.3 = ((bf16[48,29,128]{2,1,0:T(8,128)(2,1)}), bf16[48,29,128]{2,1,0:T(8,128)(2,1)S(1)}, u32[]{:S(2)}, u32[]{:S(2)}) async-start(bf16[48,29,128]{2,1,0:T(8,128)(2,1)} %pad_maximum_fusion), calls=%async_computation.3 | async-start | bytes 786432 | tf_op jit(solution)/shard_map/all_to_all | solution.py:386
  135.3 14.9 %all-to-all-start.4 = ((bf16[16,29,128]{2,1,0:T(8,128)(2,1)}), bf16[16,29,128]{2,1,0:T(8,128)(2,1)S(1)}, u32[]{:S(2)}, u32[]{:S(2)}) async-start(bf16[16,29,128]{2,1,0:T(8,128)(2,1)} %broadcast_in_dim.28), calls=%async_computation.4 | async-start | bytes 262144 | tf_op jit(solution)/shard_map/all_to_all | solution.py:386

commit v3 on v2

--- a/solution.py
+++ b/solution.py
@@ -14,6 +14,7 @@
 SPAN_LIMIT = 80.0
 PACK = 4
 GROUP = 4
+NEAR = 4
 UNROLL = 4
 f32 = jnp.float32
 bf16 = jnp.bfloat16
@@ -34,9 +35,9 @@
 
 
 def mixer_kernel(
-    came_hbm, wu_ref, off_ref, ex_ref, q_hbm, k_hbm, v_hbm,
-    goes_hbm, bias_ref,
-    low_s, do_ref, q_ref, k_ref, v_ref, goes_ref, wbig, parts, b_s, pre_s, qp_s, kf_s, st_s,
+    came_hbm, wu_hbm, off_hbm, ex_hbm, q_hbm, k_hbm, v_hbm,
+    goes_hbm, bias_hbm,
+    wu_ref, off_ref, ex_ref, bias_ref, low_s, do_ref, q_ref, k_ref, v_ref, goes_ref, wbig, parts, b_s, pre_s, qp_s, kf_s, st_s,
     pt_s, dqi_s, dki_s, x_s, y_s, e_s, gate_s, sems,
 ):
     blocks = q_ref.shape[0]
@@ -49,6 +50,9 @@
 
     copies = [
         pltpu.make_async_copy(came_hbm.at[:, halves * BLOCK :], low_s, sems.at[0]),
+        pltpu.make_async_copy(wu_hbm, wu_ref, sems.at[8]),
+        pltpu.make_async_copy(off_hbm, off_ref, sems.at[9]),
+        pltpu.make_async_copy(ex_hbm, ex_ref, sems.at[10]),
         pltpu.make_async_copy(q_hbm, q_ref, sems.at[1]),
         pltpu.make_async_copy(k_hbm, k_ref, sems.at[2]),
         pltpu.make_async_copy(came_hbm.at[:, : halves * BLOCK], do_ref, sems.at[3]),
@@ -71,9 +75,10 @@
     col_id = lax.broadcasted_iota(jnp.int32, (BLOCK, BLOCK), 1)
 
     wbig[...] = jnp.zeros(wbig.shape, bf16)
+    for copy in copies[:4]:
+        copy.wait()
     for p in range(PACK):
         wbig[RANK * p : RANK * (p + 1), lanes * p : lanes * (p + 1)] = wu_ref[...]
-    copies[0].wait()
     low = low_s[...].reshape(blocks * rows, lanes)
     raw = mm(low, wbig[...])
     offs = off_ref[...]
@@ -103,7 +108,7 @@
         centre = b[middle : middle + 1]
         span = jnp.maximum(span, jnp.maximum(b[:1] - centre, centre - b[BLOCK - 1 :]))
     narrow = jnp.max(span) < SPAN_LIMIT
-    for copy in copies[1:]:
+    for copy in copies[4:]:
         copy.wait()
 
     @pl.when(narrow)
@@ -289,6 +294,9 @@
         goes_ref.at[:, first:], goes_hbm.at[:, first:], sems.at[7]
     )
     out_rest.start()
+    out_bias = pltpu.make_async_copy(bias_ref, bias_hbm, sems.at[11])
+    out_bias.start()
+    out_bias.wait()
     out_q.wait()
     out_kv.wait()
     out_rest.wait()
@@ -346,16 +354,19 @@
     height = 4 * BLOCK + rows + 2 * RANK // blocks
     vmem = pltpu.VMEM
     anywhere = pl.BlockSpec(memory_space=pl.ANY)
-    inside = pl.BlockSpec(memory_space=pltpu.VMEM)
     return pl.pallas_call(
         mixer_kernel,
         out_shape=(
             jax.ShapeDtypeStruct((blocks, height, A), bf16),
             jax.ShapeDtypeStruct((2, A), bf16),
         ),
-        in_specs=[anywhere, inside, inside, inside, anywhere, anywhere, anywhere],
-        out_specs=[anywhere, inside],
+        in_specs=[anywhere] * 7,
+        out_specs=[anywhere] * 2,
         scratch_shapes=[
+            vmem((RANK, A), bf16),
+            vmem((1, A), f32),
+            vmem((BLOCK, blocks), f32),
+            vmem((2, A), bf16),
             vmem((blocks, rows, A), bf16),
             vmem((blocks, V // A * BLOCK, A), bf16),
             vmem((blocks, BLOCK, A), bf16),
@@ -376,14 +387,16 @@
             vmem((blocks, BLOCK, A), f32),
             vmem((blocks, 1, A), f32),
             vmem((blocks * rows, PACK * A), bf16),
-            pltpu.SemaphoreType.DMA((8,)),
+            pltpu.SemaphoreType.DMA((12,)),
         ],
         name="mixer",
     )(came, wu, off, ex, q, k, v)
 
 
-def exchanged(tensor, axis):
-    return lax.all_to_all(tensor, axis, split_axis=0, concat_axis=0, tiled=True)
+def exchanged(tensor, axis, groups=None):
+    return lax.all_to_all(
+        tensor, axis, split_axis=0, concat_axis=0, tiled=True, axis_index_groups=groups
+    )
 
 
 def everyones(tensor, axis):
@@ -462,12 +475,28 @@
     whole = in_rows(whole.astype(bf16).reshape(dp, part, R))
     n_whole = whole.shape[1]
     own = jnp.concatenate([up.astype(bf16), bias], axis=0)
-    second = exchanged(
-        jnp.concatenate([whole, jnp.broadcast_to(own, (dp, *own.shape))], axis=1), "dp"
-    )
-    second = jnp.sum(second.astype(f32), axis=0)
-    second = jnp.concatenate(
-        [second[:-2].astype(bf16), *two_parts(second[-2:-1] + second[-1:])], axis=0
+    near, far = NEAR, dp // NEAR
+    near_groups = [[z * near + x for x in range(near)] for z in range(far)]
+    far_groups = [[z * near + x for z in range(far)] for x in range(near)]
+
+    def shared(pieces, rest, groups):
+        count = len(groups[0])
+        payload = jnp.concatenate(
+            [pieces.reshape(count, -1, A), jnp.broadcast_to(rest, (count, *rest.shape))], axis=1
+        )
+        return jnp.sum(exchanged(payload, "dp", groups).astype(f32), axis=0)
+
+    def bias_kept(total):
+        return jnp.concatenate(
+            [total[:-2].astype(bf16), *two_parts(total[-2:-1] + total[-1:])], axis=0
+        )
+
+    whole = whole.reshape(far, near, n_whole, A).transpose(1, 0, 2, 3)
+    second = bias_kept(shared(whole, own, near_groups))
+    second = bias_kept(
+        shared(
+            second[: far * n_whole].reshape(far, n_whole, A), second[far * n_whole :], far_groups
+        )
     )
     third = everyones(second, "sp").astype(f32)
     down_grad = jnp.sum(third[:, :n_whole], axis=0).reshape(-1)[: part * R].reshape(part, R)

time: 153 us -> 148 us (0.967)
  waiting for transfers between devices: 35.3 us -> 25.3 us
  blocking collectives: 63.3 us -> 71.4 us
    all_to_all x3, waiting for transfers between devices: 35.3 us -> 25.3 us  [exchanged(): lax.all_to_all(tensor, axis, split_axis=0, concat_axis=0, tiled=True, axi...]
    all_to_all x2 -> x3, blocking collectives: 63.3 us -> 71.4 us  [exchanged(): lax.all_to_all(tensor, axis, split_axis=0, concat_axis=0, tiled=True, axi...]
  transfers between devices with their start and end apart: 3 -> 3, of which waited for: 3 -> 3; matrix products, arithmetic and copies ran while one was open for 3% -> 4% of each run, Pallas kernels for 2% -> 2%
where the time goes in v3:
time: 148 us
  blocking collectives  71.4 us (48%)
  starting transfers between devices  27.8 us (19%)
  waiting for transfers between devices  25.3 us (17%)
  local copies, waits for them, and re-layouts  10.5 us (7%)
  Pallas kernels  9.48 us (6%)
  other arithmetic  1.6 us (1%)
    all_to_all x3, blocking collectives, exchanged(): lax.all_to_all(tensor, axis, split_axis=0, concat_axis=0, tiled=True, axi...  71.4 us
    all_to_all x3, starting transfers between devices, exchanged(): lax.all_to_all(tensor, axis, split_axis=0, concat_axis=0, tiled=True, axi...  27.8 us
    all_to_all x3, waiting for transfers between devices, exchanged(): lax.all_to_all(tensor, axis, split_axis=0, concat_axis=0, tiled=True, axi...  25.3 us
    pallas_call x1, Pallas kernels, mixer(): pl.pallas_call(mixer_kernel, out_shape=(jax.ShapeDtypeStruct((blocks, hei...  6.92 us
  transfers between devices with their start and end apart: 3, of which 3 were waited for; matrix products, arithmetic and copies ran while one was open for 4% of the time, Pallas kernels for 2%

profile of v3, /device:TPU:1, one launch (start us, length us, event | category | flops | bytes accessed | tf_op | source)
XLA Modules:
  0.0 147.9 jit_solution(4892718141533173548)
XLA Ops:
  0.6 0.0 copy-start
  0.6 0.8 copy.56
  1.5 0.1 reshape.99
  1.6 0.7 broadcast_in_dim.27
  2.3 18.8 %all-to-all-start = ((bf16[48,11,128]{2,1,0:T(8,128)(2,1)}), bf16[48,11,128]{2,1,0:T(8,128)(2,1)S(1)}, u32[]{:S(2)}, u32[]{:S(2)}) async-start(bf16[48,11,128]{2,1,0:T(8,128)(2,1)} %broadcast_in_dim.27), calls=%async_computation | async-start | bytes 393216 | tf_op jit(solution)/shard_map/all_to_all | solution.py:397
  21.2 2.6 %prepare.1 = (bf16[16,144,128]{2,1,0:T(8,128)(2,1)}, bf16[32,128]{1,0:T(8,128)(2,1)}, f32[1,128]{1,0:T(1,128)}, f32[64,16]{1,0:T(8,128)}) custom-call(s32[1]{0:T(128)} %bitcast.head_ref, bf16[2,64,2048]{2,1,0:T(8,128)(2,1)} %adj_ref.1, bf16[32,1024]{1,0:T(8,128)(2,1)} %wide_ref.1, f32[1,1024]{1,0:T(1,128)} %bitcast.90, f32[1,1024]{1,0:T(1,128)} %ex_ref.1), custom_call_target="tpu_custom_call" | custom-call | tf_op jit(solution)/shard_map/prepare/pallas_call | solution.py:337
  23.7 11.4 %all-to-all-done = bf16[48,11,128]{2,1,0:T(8,128)(2,1)S(1)} async-done(((bf16[48,11,128]{2,1,0:T(8,128)(2,1)}), bf16[48,11,128]{2,1,0:T(8,128)(2,1)S(1)}, u32[]{:S(2)}, u32[]{:S(2)}) %all-to-all-start) | async-done | bytes 135200 | tf_op jit(solution)/shard_map/all_to_all | solution.py:397
  35.1 0.0 copy-start.1
  35.1 0.5 reshape.102
  35.6 0.0 copy-done
  35.6 0.3 fusion.1
  35.9 0.1 copy.57
  36.1 0.1 broadcast_in_dim.28
  36.2 0.0 copy-done.1
  36.2 28.8 %all_to_all.30.came_hbm = bf16[16,144,128]{2,1,0:T(8,128)(2,1)} all-to-all(bf16[16,144,128]{2,1,0:T(8,128)(2,1)S(1)} %constant_dynamic-update-slice_fusion), channel_id=1, replica_groups=mesh['sp'=16,'dp'=48] {'sp'}, dimensions={0} | all-to-all | bytes 1179648 | tf_op jit(solution)/shard_map/all_to_all | solution.py:397
  65.0 6.9 %mixer.1 = (bf16[16,276,128]{2,1,0:T(8,128)(2,1)}, bf16[2,128]{1,0:T(2,128)(2,1)}) custom-call(bf16[16,144,128]{2,1,0:T(8,128)(2,1)} %all_to_all.30.came_hbm, bf16[32,128]{1,0:T(8,128)(2,1)} %get-tuple-element.14.wu_hbm, f32[1,128]{1,0:T(1,128)} %get-tuple-element.15.off_hbm, f32[64,16]{1,0:T(8,128)} %get-tuple-element.16.ex_hbm, ...), custom_call_target="tpu_custom_call" | custom-call | tf_op jit(solution)/shard_map/mixer/pallas_call | solution.py:357
  71.9 34.6 %all_to_all.31 = bf16[16,276,128]{2,1,0:T(8,128)(2,1)S(1)} all-to-all(bf16[16,276,128]{2,1,0:T(8,128)(2,1)} %get-tuple-element.17), channel_id=1, replica_groups=mesh['sp'=16,'dp'=48] {'sp'}, dimensions={0} | all-to-all | bytes 2260992 | tf_op jit(solution)/shard_map/all_to_all | solution.py:397
  106.5 0.1 convert_element_type.65
  106.6 0.2 fusion
  106.9 0.0 copy-start.2
  106.9 0.3 copy.64
  107.2 0.3 reshape_reshape.6
  107.5 0.1 reshape_reshape.7
  107.6 0.1 copy.65
  107.7 0.0 copy-done.2
  107.7 0.1 pad_maximum_fusion
  107.9 8.1 %all_to_all.32 = bf16[4,150,128]{2,1,0:T(8,128)(2,1)S(1)} all-to-all(bf16[4,150,128]{2,1,0:T(8,128)(2,1)S(1)} %copy.66), channel_id=1, replica_groups={{0,1,2,3},{4,5,6,7},{8,9,10,11},{12,13,14,15},{16,17,18,19},{20,21,22,2..., dimensions={0} | all-to-all | bytes 307200 | tf_op jit(solution)/shard_map/all_to_all | solution.py:397
  116.1 0.7 pad_maximum_fusion.1
  116.8 3.5 %all-to-all-start.4 = ((bf16[12,29,128]{2,1,0:T(8,128)(2,1)}), bf16[12,29,128]{2,1,0:T(8,128)(2,1)S(1)}, u32[]{:S(2)}, u32[]{:S(2)}) async-start(bf16[12,29,128]{2,1,0:T(8,128)(2,1)} %pad_maximum_fusion.1), calls=%async_computation.4 | async-start | bytes 196608 | tf_op jit(solution)/shard_map/all_to_all | solution.py:397
  120.3 0.4 convolution_convert_fusion
  120.7 1.1 copy.63
  121.8 8.5 %all-to-all-done.4 = bf16[12,29,128]{2,1,0:T(8,128)(2,1)S(1)} async-done(((bf16[12,29,128]{2,1,0:T(8,128)(2,1)}), bf16[12,29,128]{2,1,0:T(8,128)(2,1)S(1)}, u32[]{:S(2)}, u32[]{:S(2)}) %all-to-all-start.4) | async-done | bytes 89120 | tf_op jit(solution)/shard_map/all_to_all | solution.py:397
  130.4 0.7 broadcast_in_dim.32
  131.1 5.4 %all-to-all-start.5 = ((bf16[16,29,128]{2,1,0:T(8,128)(2,1)}), bf16[16,29,128]{2,1,0:T(8,128)(2,1)S(1)}, u32[]{:S(2)}, u32[]{:S(2)}) async-start(bf16[16,29,128]{2,1,0:T(8,128)(2,1)} %broadcast_in_dim.32), calls=%async_computation.5 | async-start | bytes 262144 | tf_op jit(solution)/shard_map/all_to_all | solution.py:397
  136.5 0.2 copy.60
  136.7 0.8 reshape.112
  137.5 0.2 copy.59
  137.7 0.8 reshape.110
  138.6 0.5 copy.61
  139.1 1.2 reshape.114
  140.3 5.4 %all-to-all-done.5 = bf16[16,29,128]{2,1,0:T(8,128)(2,1)S(1)} async-done(((bf16[16,29,128]{2,1,0:T(8,128)(2,1)}), bf16[16,29,128]{2,1,0:T(8,128)(2,1)S(1)}, u32[]{:S(2)}, u32[]{:S(2)}) %all-to-all-start.5) | async-done | bytes 118816 | tf_op jit(solution)/shard_map/all_to_all | solution.py:397
  145.8 0.1 copy.68
  145.9 0.7 copy.76
  146.6 0.1 slice.86
  146.6 0.7 copy.69
  147.3 0.6 reduce_sum.59
  (32 shorter events, 0.5 us)
Async XLA Ops:
  0.6 35.0 %copy-start = (bf16[2,64,2064]{2,1,0:T(8,128)(2,1)S(1)}, bf16[2,64,2064]{2,1,0:T(8,128)(2,1)}, u32[]{:S(2)}) copy-start(bf16[2,64,2064]{2,1,0:T(8,128)(2,1)} %param.9) | copy-start | bytes 1585156
  2.3 32.8 %all-to-all-start = ((bf16[48,11,128]{2,1,0:T(8,128)(2,1)}), bf16[48,11,128]{2,1,0:T(8,128)(2,1)S(1)}, u32[]{:S(2)}, u32[]{:S(2)}) async-start(bf16[48,11,128]{2,1,0:T(8,128)(2,1)} %broadcast_in_dim.27), calls=%async_computation | async-start | bytes 393216 | tf_op jit(solution)/shard_map/all_to_all | solution.py:397
  35.1 1.1 copy-start.1
  106.9 0.8 copy-start.2
  116.8 13.5 %all-to-all-start.4 = ((bf16[12,29,128]{2,1,0:T(8,128)(2,1)}), bf16[12,29,128]{2,1,0:T(8,128)(2,1)S(1)}, u32[]{:S(2)}, u32[]{:S(2)}) async-start(bf16[12,29,128]{2,1,0:T(8,128)(2,1)} %pad_maximum_fusion.1), calls=%async_computation.4 | async-start | bytes 196608 | tf_op jit(solution)/shard_map/all_to_all | solution.py:397
  131.1 14.6 %all-to-all-start.5 = ((bf16[16,29,128]{2,1,0:T(8,128)(2,1)}), bf16[16,29,128]{2,1,0:T(8,128)(2,1)S(1)}, u32[]{:S(2)}, u32[]{:S(2)}) async-start(bf16[16,29,128]{2,1,0:T(8,128)(2,1)} %broadcast_in_dim.32), calls=%async_computation.5 | async-start | bytes 262144 | tf_op jit(solution)/shard_map/all_to_all | solution.py:397

commit v4 on v3

--- a/solution.py
+++ b/solution.py
@@ -463,7 +463,8 @@
     low_grad = jnp.sum(first[:, :rows].reshape(seqs, HEADS, rows, A), axis=1).astype(bf16)
     low_grad = low_grad.reshape(seqs, rows, PACK, R).transpose(0, 2, 1, 3).reshape(tokens, R)
     up = first[:, rows : rows + share] + first[:, rows + share : rows + 2 * share]
-    up = jnp.sum(up.reshape(seqs, HEADS * share, A), axis=0)
+    up = jnp.sum(up.reshape(seqs, HEADS, share, A), axis=0)
+    up = up.transpose(1, 0, 2).reshape(share * HEADS, A)
 
     def to_tokens(start, pieces):
         block = returned[:, start * BLOCK : (start + pieces) * BLOCK]
@@ -500,13 +501,10 @@
     )
     third = everyones(second, "sp").astype(f32)
     down_grad = jnp.sum(third[:, :n_whole], axis=0).reshape(-1)[: part * R].reshape(part, R)
-    up_grad = (
-        third[:, n_whole:-2]
-        .reshape(sp, HEADS, share, A)
-        .transpose(0, 2, 1, 3)
-        .reshape(R, HEADS * A)
-    )
-    bias_grad = jnp.sum((third[:, -2] + third[:, -1]).reshape(seqs, HEADS * A), axis=0)
+    up_grad = third[:, n_whole:-2].reshape(R, HEADS * A)
+    bias_grad = jnp.sum(
+        (third[:, -2] + third[:, -1]).reshape(seqs, HEADS, A), axis=0
+    ).reshape(-1)
     return (
         to_tokens(0, 1),
         to_tokens(1, 1),

time: 148 us -> 148 us (level)
  no operation moved by 1% of the time
where the time goes in v4:
time: 148 us
  blocking collectives  71.4 us (48%)
  starting transfers between devices  27.8 us (19%)
  waiting for transfers between devices  25.3 us (17%)
  local copies, waits for them, and re-layouts  10.4 us (7%)
  Pallas kernels  9.48 us (6%)
  other arithmetic  1.58 us (1%)
    all_to_all x3, blocking collectives, exchanged(): lax.all_to_all(tensor, axis, split_axis=0, concat_axis=0, tiled=True, axi...  71.4 us
    all_to_all x3, starting transfers between devices, exchanged(): lax.all_to_all(tensor, axis, split_axis=0, concat_axis=0, tiled=True, axi...  27.8 us
    all_to_all x3, waiting for transfers between devices, exchanged(): lax.all_to_all(tensor, axis, split_axis=0, concat_axis=0, tiled=True, axi...  25.3 us
    pallas_call x1, Pallas kernels, mixer(): pl.pallas_call(mixer_kernel, out_shape=(jax.ShapeDtypeStruct((blocks, hei...  6.92 us
  transfers between devices with their start and end apart: 3, of which 3 were waited for; matrix products, arithmetic and copies ran while one was open for 4% of the time, Pallas kernels for 2%

profile of v4, /device:TPU:1, one launch (start us, length us, event | category | flops | bytes accessed | tf_op | source)
XLA Modules:
  0.0 147.8 jit_solution(3544774430805943888)
XLA Ops:
  0.6 0.0 copy-start
  0.6 0.8 copy.66
  1.5 0.1 reshape.101
  1.6 0.7 broadcast_in_dim.27
  2.3 18.8 %all-to-all-start = ((bf16[48,11,128]{2,1,0:T(8,128)(2,1)}), bf16[48,11,128]{2,1,0:T(8,128)(2,1)S(1)}, u32[]{:S(2)}, u32[]{:S(2)}) async-start(bf16[48,11,128]{2,1,0:T(8,128)(2,1)} %broadcast_in_dim.27), calls=%async_computation | async-start | bytes 393216 | tf_op jit(solution)/shard_map/all_to_all | solution.py:397
  21.2 2.6 %prepare.1 = (bf16[16,144,128]{2,1,0:T(8,128)(2,1)}, bf16[32,128]{1,0:T(8,128)(2,1)}, f32[1,128]{1,0:T(1,128)}, f32[64,16]{1,0:T(8,128)}) custom-call(s32[1]{0:T(128)} %bitcast.head_ref, bf16[2,64,2048]{2,1,0:T(8,128)(2,1)} %adj_ref.1, bf16[32,1024]{1,0:T(8,128)(2,1)} %wide_ref.1, f32[1,1024]{1,0:T(1,128)} %bitcast.88, f32[1,1024]{1,0:T(1,128)} %ex_ref.1), custom_call_target="tpu_custom_call" | custom-call | tf_op jit(solution)/shard_map/prepare/pallas_call | solution.py:337
  23.7 11.4 %all-to-all-done = bf16[48,11,128]{2,1,0:T(8,128)(2,1)S(1)} async-done(((bf16[48,11,128]{2,1,0:T(8,128)(2,1)}), bf16[48,11,128]{2,1,0:T(8,128)(2,1)S(1)}, u32[]{:S(2)}, u32[]{:S(2)}) %all-to-all-start) | async-done | bytes 135200 | tf_op jit(solution)/shard_map/all_to_all | solution.py:397
  35.1 0.0 copy-start.1
  35.1 0.5 reshape.104
  35.6 0.0 copy-done
  35.6 0.3 fusion.1
  35.9 0.1 copy.67
  36.1 0.1 broadcast_in_dim.28
  36.2 0.0 copy-done.1
  36.2 28.8 %all_to_all.30.came_hbm = bf16[16,144,128]{2,1,0:T(8,128)(2,1)} all-to-all(bf16[16,144,128]{2,1,0:T(8,128)(2,1)S(1)} %constant_dynamic-update-slice_fusion), channel_id=1, replica_groups=mesh['sp'=16,'dp'=48] {'sp'}, dimensions={0} | all-to-all | bytes 1179648 | tf_op jit(solution)/shard_map/all_to_all | solution.py:397
  65.0 6.9 %mixer.1 = (bf16[16,276,128]{2,1,0:T(8,128)(2,1)}, bf16[2,128]{1,0:T(2,128)(2,1)}) custom-call(bf16[16,144,128]{2,1,0:T(8,128)(2,1)} %all_to_all.30.came_hbm, bf16[32,128]{1,0:T(8,128)(2,1)} %get-tuple-element.14.wu_hbm, f32[1,128]{1,0:T(1,128)} %get-tuple-element.15.off_hbm, f32[64,16]{1,0:T(8,128)} %get-tuple-element.16.ex_hbm, ...), custom_call_target="tpu_custom_call" | custom-call | tf_op jit(solution)/shard_map/mixer/pallas_call | solution.py:357
  71.9 34.6 %all_to_all.31 = bf16[16,276,128]{2,1,0:T(8,128)(2,1)S(1)} all-to-all(bf16[16,276,128]{2,1,0:T(8,128)(2,1)} %get-tuple-element.17), channel_id=1, replica_groups=mesh['sp'=16,'dp'=48] {'sp'}, dimensions={0} | all-to-all | bytes 2260992 | tf_op jit(solution)/shard_map/all_to_all | solution.py:397
  106.6 0.1 convert_element_type.71
  106.7 0.2 fusion
  106.9 0.0 copy-start.2
  106.9 0.3 copy.74
  107.2 0.3 reshape_reshape.6
  107.5 0.1 reshape_reshape.7
  107.7 0.1 copy.75
  107.7 0.0 copy-done.2
  107.8 0.1 pad_maximum_fusion
  107.9 8.1 %all_to_all.32 = bf16[4,150,128]{2,1,0:T(8,128)(2,1)S(1)} all-to-all(bf16[4,150,128]{2,1,0:T(8,128)(2,1)S(1)} %copy.77), channel_id=1, replica_groups={{0,1,2,3},{4,5,6,7},{8,9,10,11},{12,13,14,15},{16,17,18,19},{20,21,22,2..., dimensions={0} | all-to-all | bytes 307200 | tf_op jit(solution)/shard_map/all_to_all | solution.py:397
  116.1 0.7 pad_maximum_fusion.1
  116.8 3.5 %all-to-all-start.4 = ((bf16[12,29,128]{2,1,0:T(8,128)(2,1)}), bf16[12,29,128]{2,1,0:T(8,128)(2,1)S(1)}, u32[]{:S(2)}, u32[]{:S(2)}) async-start(bf16[12,29,128]{2,1,0:T(8,128)(2,1)} %pad_maximum_fusion.1), calls=%async_computation.4 | async-start | bytes 196608 | tf_op jit(solution)/shard_map/all_to_all | solution.py:397
  120.3 0.4 convolution_convert_fusion
  120.7 1.1 copy.73
  121.8 8.5 %all-to-all-done.4 = bf16[12,29,128]{2,1,0:T(8,128)(2,1)S(1)} async-done(((bf16[12,29,128]{2,1,0:T(8,128)(2,1)}), bf16[12,29,128]{2,1,0:T(8,128)(2,1)S(1)}, u32[]{:S(2)}, u32[]{:S(2)}) %all-to-all-start.4) | async-done | bytes 89120 | tf_op jit(solution)/shard_map/all_to_all | solution.py:397
  130.4 0.7 broadcast_in_dim.32
  131.1 5.4 %all-to-all-start.5 = ((bf16[16,29,128]{2,1,0:T(8,128)(2,1)}), bf16[16,29,128]{2,1,0:T(8,128)(2,1)S(1)}, u32[]{:S(2)}, u32[]{:S(2)}) async-start(bf16[16,29,128]{2,1,0:T(8,128)(2,1)} %broadcast_in_dim.32), calls=%async_computation.5 | async-start | bytes 262144 | tf_op jit(solution)/shard_map/all_to_all | solution.py:397
  136.5 0.2 copy.70
  136.7 0.8 reshape.114
  137.5 0.2 copy.69
  137.7 0.8 reshape.112
  138.6 0.5 copy.71
  139.1 1.2 reshape.116
  140.3 5.4 %all-to-all-done.5 = bf16[16,29,128]{2,1,0:T(8,128)(2,1)S(1)} async-done(((bf16[16,29,128]{2,1,0:T(8,128)(2,1)}), bf16[16,29,128]{2,1,0:T(8,128)(2,1)S(1)}, u32[]{:S(2)}, u32[]{:S(2)}) %all-to-all-start.5) | async-done | bytes 118816 | tf_op jit(solution)/shard_map/all_to_all | solution.py:397
  145.8 0.7 reshape.123
  146.5 0.6 bitcast_reduce_fusion.1
  147.1 0.1 slice.86
  147.1 0.7 copy.78
  (32 shorter events, 0.5 us)
Async XLA Ops:
  0.6 35.0 %copy-start = (bf16[2,64,2064]{2,1,0:T(8,128)(2,1)S(1)}, bf16[2,64,2064]{2,1,0:T(8,128)(2,1)}, u32[]{:S(2)}) copy-start(bf16[2,64,2064]{2,1,0:T(8,128)(2,1)} %param.9) | copy-start | bytes 1585156
  2.3 32.8 %all-to-all-start = ((bf16[48,11,128]{2,1,0:T(8,128)(2,1)}), bf16[48,11,128]{2,1,0:T(8,128)(2,1)S(1)}, u32[]{:S(2)}, u32[]{:S(2)}) async-start(bf16[48,11,128]{2,1,0:T(8,128)(2,1)} %broadcast_in_dim.27), calls=%async_computation | async-start | bytes 393216 | tf_op jit(solution)/shard_map/all_to_all | solution.py:397
  35.1 1.1 copy-start.1
  106.9 0.8 copy-start.2
  116.8 13.5 %all-to-all-start.4 = ((bf16[12,29,128]{2,1,0:T(8,128)(2,1)}), bf16[12,29,128]{2,1,0:T(8,128)(2,1)S(1)}, u32[]{:S(2)}, u32[]{:S(2)}) async-start(bf16[12,29,128]{2,1,0:T(8,128)(2,1)} %pad_maximum_fusion.1), calls=%async_computation.4 | async-start | bytes 196608 | tf_op jit(solution)/shard_map/all_to_all | solution.py:397
  131.1 14.6 %all-to-all-start.5 = ((bf16[16,29,128]{2,1,0:T(8,128)(2,1)}), bf16[16,29,128]{2,1,0:T(8,128)(2,1)S(1)}, u32[]{:S(2)}, u32[]{:S(2)}) async-start(bf16[16,29,128]{2,1,0:T(8,128)(2,1)} %broadcast_in_dim.32), calls=%async_computation.5 | async-start | bytes 262144 | tf_op jit(solution)/shard_map/all_to_all | solution.py:397

commit v5 on v4

--- a/solution.py
+++ b/solution.py
@@ -38,7 +38,7 @@
     came_hbm, wu_hbm, off_hbm, ex_hbm, q_hbm, k_hbm, v_hbm,
     goes_hbm, bias_hbm,
     wu_ref, off_ref, ex_ref, bias_ref, low_s, do_ref, q_ref, k_ref, v_ref, goes_ref, wbig, parts, b_s, pre_s, qp_s, kf_s, st_s,
-    pt_s, dqi_s, dki_s, x_s, y_s, e_s, gate_s, sems,
+    pt_s, dqi_s, dki_s, x_s, e_s, gate_s, sems,
 ):
     blocks = q_ref.shape[0]
     rows = BLOCK // PACK
@@ -181,6 +181,10 @@
 
             lax.fori_loop(0, blocks // GROUP, within, 0)
 
+    def split(n, first, terms):
+        for i, part in enumerate(three_parts(terms), first):
+            parts[BLOCK * i : BLOCK * (i + 1), lanes * n : lanes * (n + 1)] = part
+
     def spread(tensor):
         zero = jnp.zeros((BLOCK, lanes), tensor.dtype)
         return jnp.concatenate(
@@ -210,13 +214,18 @@
             n = at + m
             st_s[n] = state
             dq = mm(do[BLOCK * m : BLOCK * (m + 1)], state.astype(bf16))
-            x_s[n] = x_s[n] + qp[m].astype(f32) * dq
+            split(n, 0, x_s[n] + qp[m].astype(f32) * dq)
+            pre = pre_s[n]
+            e = jnp.exp(-jnp.abs(pre))
+            pre_s[n] = jnp.where(pre >= 0.0, e, 1.0) / (1.0 + e)
             goes_ref[n, :BLOCK] = ((dqi_s[n] + dq * grow[m]) * scale).astype(bf16)
             state = state * fade[m] + added[:, lanes * m : lanes * (m + 1)]
         return state
 
     zero = jnp.zeros((PAYLOAD_WIDTH, lanes), f32)
-    lax.fori_loop(0, blocks // GROUP, forward, zero, unroll=UNROLL)
+    state = zero
+    for g in range(blocks // GROUP):
+        state = forward(g, state)
     out_q = pltpu.make_async_copy(
         goes_ref.at[:, :BLOCK], goes_hbm.at[:, :BLOCK], sems.at[5]
     )
@@ -243,32 +252,26 @@
                 goes_ref[n, BLOCK * (2 + i) : BLOCK * (3 + i)] = dv[
                     :, lanes * i : lanes * (i + 1)
                 ]
-            y_s[n] = kf.astype(f32) * dk
+            split(n, 3, kf.astype(f32) * dk)
             e_s[n] = fade[m] * jnp.sum(st_s[n] * dstate, axis=0, keepdims=True)
             dstate = dstate * fade[m] + added[:, lanes * m : lanes * (m + 1)]
         return dstate
 
-    lax.fori_loop(0, blocks // GROUP, backward, zero, unroll=UNROLL)
+    dstate = zero
+    for i in range(blocks // GROUP):
+        dstate = backward(i, dstate)
     out_kv = pltpu.make_async_copy(
         goes_ref.at[:, BLOCK : 4 * BLOCK], goes_hbm.at[:, BLOCK : 4 * BLOCK], sems.at[6]
     )
     out_kv.start()
 
-    for n in range(blocks):
-        for i, part in enumerate(three_parts(x_s[n])):
-            parts[BLOCK * i : BLOCK * (i + 1), lanes * n : lanes * (n + 1)] = part
-        for i, part in enumerate(three_parts(y_s[n])):
-            parts[BLOCK * (3 + i) : BLOCK * (4 + i), lanes * n : lanes * (n + 1)] = part
     upper = (row_id <= col_id).astype(bf16)
     before = (row_id > col_id).astype(bf16)
     ddecay = mm(jnp.concatenate([upper] * 3 + [before] * 3, axis=1), parts[...])
     bias = jnp.zeros((1, lanes), f32)
     for n in range(blocks):
-        pre = pre_s[n]
-        e = jnp.exp(-jnp.abs(pre))
-        slope = jnp.where(pre >= 0.0, e, 1.0) / (1.0 + e)
         gate = (
-            (ddecay[:, lanes * n : lanes * (n + 1)] + e_s[n]) * slope * (1.0 / SMOOTHING)
+            (ddecay[:, lanes * n : lanes * (n + 1)] + e_s[n]) * pre_s[n] * (1.0 / SMOOTHING)
         ).astype(bf16)
         bias = bias + jnp.sum(gate.astype(f32), axis=0, keepdims=True)
         for p in range(PACK):
@@ -384,7 +387,6 @@
             vmem((blocks, BLOCK, A), f32),
             vmem((blocks, BLOCK, A), f32),
             vmem((blocks, BLOCK, A), f32),
-            vmem((blocks, BLOCK, A), f32),
             vmem((blocks, 1, A), f32),
             vmem((blocks * rows, PACK * A), bf16),
             pltpu.SemaphoreType.DMA((12,)),

time: 148 us -> 148 us (level)
  no operation moved by 1% of the time
where the time goes in v5:
time: 148 us
  blocking collectives  71.4 us (48%)
  starting transfers between devices  27.8 us (19%)
  waiting for transfers between devices  25.3 us (17%)
  local copies, waits for them, and re-layouts  10.4 us (7%)
  Pallas kernels  9.48 us (6%)
  other arithmetic  1.58 us (1%)
    all_to_all x3, blocking collectives, exchanged(): lax.all_to_all(tensor, axis, split_axis=0, concat_axis=0, tiled=True, axi...  71.4 us
    all_to_all x3, starting transfers between devices, exchanged(): lax.all_to_all(tensor, axis, split_axis=0, concat_axis=0, tiled=True, axi...  27.8 us
    all_to_all x3, waiting for transfers between devices, exchanged(): lax.all_to_all(tensor, axis, split_axis=0, concat_axis=0, tiled=True, axi...  25.3 us
    pallas_call x1, Pallas kernels, mixer(): pl.pallas_call(mixer_kernel, out_shape=(jax.ShapeDtypeStruct((blocks, hei...  6.92 us
  transfers between devices with their start and end apart: 3, of which 3 were waited for; matrix products, arithmetic and copies ran while one was open for 4% of the time, Pallas kernels for 2%

profile of v5, /device:TPU:1, one launch (start us, length us, event | category | flops | bytes accessed | tf_op | source)
XLA Modules:
  0.0 147.8 jit_solution(5189199002169369735)
XLA Ops:
  0.6 0.0 copy-start
  0.6 0.8 copy.66
  1.5 0.1 reshape.101
  1.6 0.7 broadcast_in_dim.27
  2.3 18.8 %all-to-all-start = ((bf16[48,11,128]{2,1,0:T(8,128)(2,1)}), bf16[48,11,128]{2,1,0:T(8,128)(2,1)S(1)}, u32[]{:S(2)}, u32[]{:S(2)}) async-start(bf16[48,11,128]{2,1,0:T(8,128)(2,1)} %broadcast_in_dim.27), calls=%async_computation | async-start | bytes 393216 | tf_op jit(solution)/shard_map/all_to_all | solution.py:399
  21.2 2.6 %prepare.1 = (bf16[16,144,128]{2,1,0:T(8,128)(2,1)}, bf16[32,128]{1,0:T(8,128)(2,1)}, f32[1,128]{1,0:T(1,128)}, f32[64,16]{1,0:T(8,128)}) custom-call(s32[1]{0:T(128)} %bitcast.head_ref, bf16[2,64,2048]{2,1,0:T(8,128)(2,1)} %adj_ref.1, bf16[32,1024]{1,0:T(8,128)(2,1)} %wide_ref.1, f32[1,1024]{1,0:T(1,128)} %bitcast.88, f32[1,1024]{1,0:T(1,128)} %ex_ref.1), custom_call_target="tpu_custom_call" | custom-call | tf_op jit(solution)/shard_map/prepare/pallas_call | solution.py:340
  23.7 11.4 %all-to-all-done = bf16[48,11,128]{2,1,0:T(8,128)(2,1)S(1)} async-done(((bf16[48,11,128]{2,1,0:T(8,128)(2,1)}), bf16[48,11,128]{2,1,0:T(8,128)(2,1)S(1)}, u32[]{:S(2)}, u32[]{:S(2)}) %all-to-all-start) | async-done | bytes 135200 | tf_op jit(solution)/shard_map/all_to_all | solution.py:399
  35.1 0.0 copy-start.1
  35.1 0.5 reshape.104
  35.6 0.0 copy-done
  35.6 0.3 fusion.1
  35.9 0.1 copy.67
  36.1 0.1 broadcast_in_dim.28
  36.2 0.0 copy-done.1
  36.2 28.8 %all_to_all.30.came_hbm = bf16[16,144,128]{2,1,0:T(8,128)(2,1)} all-to-all(bf16[16,144,128]{2,1,0:T(8,128)(2,1)S(1)} %constant_dynamic-update-slice_fusion), channel_id=1, replica_groups=mesh['sp'=16,'dp'=48] {'sp'}, dimensions={0} | all-to-all | bytes 1179648 | tf_op jit(solution)/shard_map/all_to_all | solution.py:399
  65.0 6.9 %mixer.1 = (bf16[16,276,128]{2,1,0:T(8,128)(2,1)}, bf16[2,128]{1,0:T(2,128)(2,1)}) custom-call(bf16[16,144,128]{2,1,0:T(8,128)(2,1)} %all_to_all.30.came_hbm, bf16[32,128]{1,0:T(8,128)(2,1)} %get-tuple-element.14.wu_hbm, f32[1,128]{1,0:T(1,128)} %get-tuple-element.15.off_hbm, f32[64,16]{1,0:T(8,128)} %get-tuple-element.16.ex_hbm, ...), custom_call_target="tpu_custom_call" | custom-call | tf_op jit(solution)/shard_map/mixer/pallas_call | solution.py:360
  71.9 34.6 %all_to_all.31 = bf16[16,276,128]{2,1,0:T(8,128)(2,1)S(1)} all-to-all(bf16[16,276,128]{2,1,0:T(8,128)(2,1)} %get-tuple-element.17), channel_id=1, replica_groups=mesh['sp'=16,'dp'=48] {'sp'}, dimensions={0} | all-to-all | bytes 2260992 | tf_op jit(solution)/shard_map/all_to_all | solution.py:399
  106.6 0.1 convert_element_type.71
  106.7 0.2 fusion
  106.9 0.0 copy-start.2
  106.9 0.3 copy.74
  107.2 0.3 reshape_reshape.6
  107.5 0.1 reshape_reshape.7
  107.7 0.1 copy.75
  107.7 0.0 copy-done.2
  107.8 0.1 pad_maximum_fusion
  107.9 8.1 %all_to_all.32 = bf16[4,150,128]{2,1,0:T(8,128)(2,1)S(1)} all-to-all(bf16[4,150,128]{2,1,0:T(8,128)(2,1)S(1)} %copy.77), channel_id=1, replica_groups={{0,1,2,3},{4,5,6,7},{8,9,10,11},{12,13,14,15},{16,17,18,19},{20,21,22,2..., dimensions={0} | all-to-all | bytes 307200 | tf_op jit(solution)/shard_map/all_to_all | solution.py:399
  116.1 0.7 pad_maximum_fusion.1
  116.8 3.5 %all-to-all-start.4 = ((bf16[12,29,128]{2,1,0:T(8,128)(2,1)}), bf16[12,29,128]{2,1,0:T(8,128)(2,1)S(1)}, u32[]{:S(2)}, u32[]{:S(2)}) async-start(bf16[12,29,128]{2,1,0:T(8,128)(2,1)} %pad_maximum_fusion.1), calls=%async_computation.4 | async-start | bytes 196608 | tf_op jit(solution)/shard_map/all_to_all | solution.py:399
  120.3 0.4 convolution_convert_fusion
  120.7 1.1 copy.73
  121.8 8.5 %all-to-all-done.4 = bf16[12,29,128]{2,1,0:T(8,128)(2,1)S(1)} async-done(((bf16[12,29,128]{2,1,0:T(8,128)(2,1)}), bf16[12,29,128]{2,1,0:T(8,128)(2,1)S(1)}, u32[]{:S(2)}, u32[]{:S(2)}) %all-to-all-start.4) | async-done | bytes 89120 | tf_op jit(solution)/shard_map/all_to_all | solution.py:399
  130.4 0.7 broadcast_in_dim.32
  131.1 5.4 %all-to-all-start.5 = ((bf16[16,29,128]{2,1,0:T(8,128)(2,1)}), bf16[16,29,128]{2,1,0:T(8,128)(2,1)S(1)}, u32[]{:S(2)}, u32[]{:S(2)}) async-start(bf16[16,29,128]{2,1,0:T(8,128)(2,1)} %broadcast_in_dim.32), calls=%async_computation.5 | async-start | bytes 262144 | tf_op jit(solution)/shard_map/all_to_all | solution.py:399
  136.5 0.2 copy.70
  136.7 0.8 reshape.114
  137.5 0.2 copy.69
  137.7 0.8 reshape.112
  138.6 0.5 copy.71
  139.1 1.2 reshape.116
  140.3 5.4 %all-to-all-done.5 = bf16[16,29,128]{2,1,0:T(8,128)(2,1)S(1)} async-done(((bf16[16,29,128]{2,1,0:T(8,128)(2,1)}), bf16[16,29,128]{2,1,0:T(8,128)(2,1)S(1)}, u32[]{:S(2)}, u32[]{:S(2)}) %all-to-all-start.5) | async-done | bytes 118816 | tf_op jit(solution)/shard_map/all_to_all | solution.py:399
  145.8 0.7 reshape.123
  146.5 0.6 bitcast_reduce_fusion.1
  147.1 0.1 slice.86
  147.1 0.7 copy.78
  (32 shorter events, 0.5 us)
Async XLA Ops:
  0.6 35.0 %copy-start = (bf16[2,64,2064]{2,1,0:T(8,128)(2,1)S(1)}, bf16[2,64,2064]{2,1,0:T(8,128)(2,1)}, u32[]{:S(2)}) copy-start(bf16[2,64,2064]{2,1,0:T(8,128)(2,1)} %param.9) | copy-start | bytes 1585156
  2.3 32.8 %all-to-all-start = ((bf16[48,11,128]{2,1,0:T(8,128)(2,1)}), bf16[48,11,128]{2,1,0:T(8,128)(2,1)S(1)}, u32[]{:S(2)}, u32[]{:S(2)}) async-start(bf16[48,11,128]{2,1,0:T(8,128)(2,1)} %broadcast_in_dim.27), calls=%async_computation | async-start | bytes 393216 | tf_op jit(solution)/shard_map/all_to_all | solution.py:399
  35.1 1.1 copy-start.1
  106.9 0.8 copy-start.2
  116.8 13.5 %all-to-all-start.4 = ((bf16[12,29,128]{2,1,0:T(8,128)(2,1)}), bf16[12,29,128]{2,1,0:T(8,128)(2,1)S(1)}, u32[]{:S(2)}, u32[]{:S(2)}) async-start(bf16[12,29,128]{2,1,0:T(8,128)(2,1)} %pad_maximum_fusion.1), calls=%async_computation.4 | async-start | bytes 196608 | tf_op jit(solution)/shard_map/all_to_all | solution.py:399
  131.1 14.6 %all-to-all-start.5 = ((bf16[16,29,128]{2,1,0:T(8,128)(2,1)}), bf16[16,29,128]{2,1,0:T(8,128)(2,1)S(1)}, u32[]{:S(2)}, u32[]{:S(2)}) async-start(bf16[16,29,128]{2,1,0:T(8,128)(2,1)} %broadcast_in_dim.32), calls=%async_computation.5 | async-start | bytes 262144 | tf_op jit(solution)/shard_map/all_to_all | solution.py:399
